TPU v7x, 32 devices: a whole 2x2x4 slice. The times are simulated.
32 devices in a mesh: st: 16 (over z, y, x), tp: 2 (over core).
Axes of the slice: x: 2, y: 2, z: 4, core: 2. Of those that a mesh axis runs over, the one named last changes fastest.
Arguments:
- tokens: bfloat16 [4096, 2048], P('st'), may hold values from -6 to 6
- store: bfloat16 [64, 64, 2048], P('st'), may hold values from -6 to 6
- passage_ids: int32 [64, 4], P('st'), may hold values from 0 to 63, as said below
- w_query: bfloat16 [2048, 2048], P(None, 'tp'), may hold values from -0.125 to 0.125
- w_key: bfloat16 [2048, 512], P(None, 'tp'), may hold values from -0.125 to 0.125
- w_value: bfloat16 [2048, 512], P(None, 'tp'), may hold values from -0.125 to 0.125
- w_ret_query: bfloat16 [2048, 1024], P(None, 'tp'), may hold values from -0.125 to 0.125
- w_ret_key: bfloat16 [2048, 1024], P(None, 'tp'), may hold values from -0.125 to 0.125
- w_ret_value: bfloat16 [2048, 2048], P(None, 'tp'), may hold values from -0.125 to 0.125
- ret_rate: float32 [8], P('tp'), may hold values from 0.003 to 0.03
- ret_gain: float32 [2048], P('tp'), may hold values from 0.1 to 1.9
- gate_logit: float32 [2048], P('tp'), may hold values from -2 to 2
- out_grad: bfloat16 [4096, 2048], P('st', 'tp'), may hold values from -6 to 6
Outputs:
- grad_tokens: bfloat16 [4096, 2048], P(('st', 'tp'))
- grad_store: bfloat16 [64, 64, 2048], P(('st', 'tp'))
- grad_key_weight: float32 [2048, 512], P(None, 'tp')
Inputs may be any that keep to these rules, and one draw needn't show every extreme that they name: `passage_ids`: passage p lies on index p // 4 of st. The rows of one device name exactly 1 passage of every owner, so the 4 passages of a block differ.
All inputs are finite; a program needn't handle non-finite values.
Results may differ from a plain program's by a relative error of at most 0.012.
Values may be sent and summed in bfloat16 or wider, within the bound.
A program may use at most 192 MiB of HBM per device.

v0:
```python
import functools

import jax
import jax.numpy as jnp
from jax import lax
from jax.experimental import pallas as pl
from jax.experimental.pallas import tpu as pltpu
from jax.sharding import PartitionSpec as P

HEAD = 256
BLK = 64
KP = 4
MOST = 1


EPSILON = 1.0


def retention_grads(query_rows, key_rows, value_rows, rates, gains, cotangent):
    length = query_rows.shape[0]
    heads = rates.shape[0]
    queries = query_rows.reshape(length, heads, -1)
    keyset = key_rows.reshape(length, heads, -1)
    values = value_rows.reshape(length, heads, -1)
    positions = jnp.arange(length, dtype=jnp.float32)
    distance = positions[:, None] - positions[None, :]
    damping = jnp.where(
        distance >= 0.0, jnp.exp(-rates[:, None, None] * jnp.maximum(distance, 0.0)), 0.0
    ) * queries.shape[-1] ** (-0.5)
    raw = jnp.einsum("thd,shd->hts", queries, keyset, preferred_element_type=jnp.float32)
    weights = (raw * damping).astype(jnp.bfloat16)
    mixed = jnp.einsum("hts,she->the", weights, values, preferred_element_type=jnp.float32)
    inverse = lax.rsqrt(jnp.mean(mixed * mixed, axis=-1, keepdims=True) + EPSILON)
    scaled = cotangent.astype(jnp.float32).reshape(length, heads, -1) * gains.reshape(heads, -1)
    inner = jnp.mean(scaled * mixed, axis=-1, keepdims=True)
    grad_mixed = (inverse * scaled - inverse * inverse * inverse * mixed * inner).astype(
        jnp.bfloat16
    )
    grad_weights = (
        jnp.einsum("the,she->hts", grad_mixed, values, preferred_element_type=jnp.float32) * damping
    ).astype(jnp.bfloat16)
    grad_first = (
        jnp.einsum("hts,shd->thd", grad_weights, keyset, preferred_element_type=jnp.float32)
        .astype(jnp.bfloat16)
        .reshape(length, -1)
    )
    grad_second = (
        jnp.einsum("hts,thd->shd", grad_weights, queries, preferred_element_type=jnp.float32)
        .astype(jnp.bfloat16)
        .reshape(length, -1)
    )
    grad_third = (
        jnp.einsum("hts,the->she", weights, grad_mixed, preferred_element_type=jnp.float32)
        .astype(jnp.bfloat16)
        .reshape(length, -1)
    )
    return (grad_first, grad_second, grad_third)


def against_rows(left, weight):
    return lax.dot_general(
        left, weight, (((1,), (1,)), ((), ())), preferred_element_type=jnp.float32
    )


def across_rows(left, right):
    return lax.dot_general(
        left, right, (((0,), (0,)), ((), ())), preferred_element_type=jnp.float32
    )


def per_device_plain(
    tokens,
    store,
    passage_ids,
    w_query,
    w_key,
    w_value,
    w_ret_query,
    w_ret_key,
    w_ret_value,
    ret_rate,
    ret_gain,
    gate_logit,
    out_grad,
):
    owners = lax.axis_size("st")
    pass_dev, plen, width = store.shape
    length = tokens.shape[0]
    kv_width = w_key.shape[1]
    kv_local = kv_width // HEAD
    group = w_query.shape[1] // HEAD // kv_local
    blocks = length // BLK
    slot_ids = passage_ids.reshape(-1)
    slot_count = slot_ids.shape[0]
    slot_owner = slot_ids // pass_dev
    slot_local = slot_ids % pass_dev
    order = jnp.arange(slot_count, dtype=jnp.int32)
    same_owner = slot_owner[:, None] == slot_owner[None, :]
    rank = jnp.sum(same_owner & (order[None, :] < order[:, None]), axis=1)
    position = slot_owner * MOST + rank
    cells = owners * MOST
    placed = jnp.arange(cells, dtype=jnp.int32)[:, None] == position[None, :]
    request = (jnp.sum(jnp.where(placed, slot_local[None, :] + 1, 0), axis=1) - 1).reshape(
        owners, MOST
    )
    incoming = lax.all_to_all(request, "st", split_axis=0, concat_axis=0, tiled=True)
    wanted = incoming.reshape(-1)
    valid = wanted >= 0
    safe = jnp.maximum(wanted, 0)
    placed_bf = placed.astype(jnp.bfloat16)
    store_rows = store.reshape(-1, width)
    nothing = jnp.zeros((), jnp.bfloat16)
    own_kv = jnp.concatenate(
        [
            jnp.dot(store_rows, w_key, preferred_element_type=jnp.float32).astype(jnp.bfloat16),
            jnp.dot(store_rows, w_value, preferred_element_type=jnp.float32).astype(jnp.bfloat16),
        ],
        axis=1,
    ).reshape(pass_dev, plen, 2 * kv_width)
    reply = jnp.where(valid[:, None, None], own_kv[safe], nothing).reshape(
        owners, MOST, plen, 2 * kv_width
    )
    arrived = lax.all_to_all(reply, "st", split_axis=0, concat_axis=0, tiled=True)
    slot_kv = (
        across_rows(placed_bf, arrived.reshape(cells, -1))
        .astype(jnp.bfloat16)
        .reshape(slot_count, plen, 2 * kv_width)
    )
    factor = HEAD ** (-0.5)
    gate = jax.nn.sigmoid(gate_logit)
    query_bf = jnp.dot(tokens, w_query, preferred_element_type=jnp.float32).astype(jnp.bfloat16)
    queries = query_bf.reshape(blocks, BLK, kv_local, group, HEAD)
    keys = slot_kv[:, :, :kv_width].reshape(blocks, KP * plen, kv_local, HEAD)
    values = slot_kv[:, :, kv_width:].reshape(blocks, KP * plen, kv_local, HEAD)
    scores = (
        jnp.einsum("btkgd,bskd->bkgts", queries, keys, preferred_element_type=jnp.float32) * factor
    )
    expo = jnp.exp(scores)
    probs = expo / jnp.sum(expo, axis=-1, keepdims=True)
    probs_bf = probs.astype(jnp.bfloat16)
    attn = jnp.einsum("bkgts,bskd->btkgd", probs_bf, values, preferred_element_type=jnp.float32)
    grad_attn = out_grad.astype(jnp.float32).reshape(
        blocks, BLK, kv_local, group, HEAD
    ) * gate.reshape(kv_local, group, HEAD)
    grad_attn_bf = grad_attn.astype(jnp.bfloat16)
    grad_probs = jnp.einsum(
        "btkgd,bskd->bkgts", grad_attn_bf, values, preferred_element_type=jnp.float32
    )
    delta = jnp.moveaxis(jnp.sum(grad_attn * attn, axis=-1), 1, 3)
    grad_scores = (probs * (grad_probs - delta[..., None]) * factor).astype(jnp.bfloat16)
    grad_query = (
        jnp.einsum("bkgts,bskd->btkgd", grad_scores, keys, preferred_element_type=jnp.float32)
        .astype(jnp.bfloat16)
        .reshape(length, -1)
    )
    grad_keys = (
        jnp.einsum("bkgts,btkgd->bskd", grad_scores, queries, preferred_element_type=jnp.float32)
        .astype(jnp.bfloat16)
        .reshape(slot_count, plen, kv_width)
    )
    grad_values = (
        jnp.einsum("bkgts,btkgd->bskd", probs_bf, grad_attn_bf, preferred_element_type=jnp.float32)
        .astype(jnp.bfloat16)
        .reshape(slot_count, plen, kv_width)
    )
    slot_grad = jnp.concatenate([grad_keys, grad_values], axis=2)
    outgoing = (
        jnp.dot(placed_bf, slot_grad.reshape(slot_count, -1), preferred_element_type=jnp.float32)
        .astype(jnp.bfloat16)
        .reshape(owners, MOST, plen, 2 * kv_width)
    )
    returned = lax.all_to_all(outgoing, "st", split_axis=0, concat_axis=0, tiled=True)
    matched = (jnp.arange(pass_dev, dtype=jnp.int32)[:, None] == wanted[None, :]).astype(
        jnp.bfloat16
    )
    passage_grad = jnp.dot(
        matched, returned.reshape(cells, -1), preferred_element_type=jnp.float32
    ).reshape(pass_dev * plen, 2 * kv_width)
    key_grad = passage_grad[:, :kv_width]
    upper = key_grad.astype(jnp.bfloat16)
    lower = (key_grad - upper.astype(jnp.float32)).astype(jnp.bfloat16)
    key_term = across_rows(store_rows, upper) + across_rows(store_rows, lower)
    grad_key_weight = lax.psum(key_term, "st")
    passage_bf = passage_grad.astype(jnp.bfloat16)
    grad_store = lax.psum_scatter(
        (
            against_rows(passage_bf[:, :kv_width], w_key)
            + against_rows(passage_bf[:, kv_width:], w_value)
        ).astype(jnp.bfloat16),
        "tp",
        scatter_dimension=0,
        tiled=True,
    ).astype(jnp.float32)
    grad_store = grad_store.astype(jnp.bfloat16).reshape(-1, plen, width)
    ret_query = jnp.dot(tokens, w_ret_query, preferred_element_type=jnp.float32).astype(
        jnp.bfloat16
    )
    ret_key = jnp.dot(tokens, w_ret_key, preferred_element_type=jnp.float32).astype(jnp.bfloat16)
    ret_value = jnp.dot(tokens, w_ret_value, preferred_element_type=jnp.float32).astype(
        jnp.bfloat16
    )
    grad_rq, grad_rk, grad_rv = retention_grads(
        ret_query, ret_key, ret_value, ret_rate, ret_gain, out_grad
    )
    total = against_rows(grad_query, w_query)
    total = total + against_rows(grad_rq, w_ret_query)
    total = total + against_rows(grad_rk, w_ret_key)
    grad_tokens = lax.psum_scatter(
        (total + against_rows(grad_rv, w_ret_value)).astype(jnp.bfloat16),
        "tp",
        scatter_dimension=0,
        tiled=True,
    )
    return (grad_tokens, grad_store, grad_key_weight)


PLANE = 4
HALVES = 2
TILE = 256
BF = jnp.bfloat16
F32 = jnp.float32
MESH = pl.DeviceIdType.MESH


def nn(a, b):
    return lax.dot_general(a, b, (((1,), (0,)), ((), ())), preferred_element_type=F32)


def nt(a, b):
    return lax.dot_general(a, b, (((1,), (1,)), ((), ())), preferred_element_type=F32)


def tn(a, b):
    return lax.dot_general(a, b, (((0,), (0,)), ((), ())), preferred_element_type=F32)


def fused_kernel(
    n,
    ids_ref,
    rate_ref,
    gain_ref,
    gate_ref,
    tokens_hbm,
    store_hbm,
    wq_hbm,
    wk_hbm,
    wv_hbm,
    wrq_hbm,
    wrk_hbm,
    wrv_hbm,
    og_hbm,
    gt_hbm,
    gs_hbm,
    gkw_hbm,
    tokens,
    store,
    wq,
    wk,
    wv,
    wrq,
    wrk,
    wrv,
    og,
    q,
    rq,
    rk,
    rv,
    gq,
    grq,
    grk,
    grv,
    total,
    gt,
    gt_in,
    gs,
    gs_in,
    own_kv,
    req_out,
    req_in,
    kv_out,
    kv_in,
    stage_k,
    stage_v,
    gk_out,
    gv_out,
    gk_in,
    gv_in,
    pk,
    pv,
    slices,
    pk_in,
    p1_sum,
    p2_in,
    kg,
    owner_of,
    slot_of,
    load_sem,
    out_sem,
    tp_send,
    tp_recv,
    req_send,
    req_recv,
    kv_send,
    kv_recv,
    gk_send,
    gk_recv,
    gv_send,
    gv_recv,
    p1_send,
    p1_recv,
    pk_send,
    pk_recv,
    p2_send,
    p2_recv,
    p3_send,
    p3_recv,
    p4_send,
    p4_recv,
):
    me = lax.axis_index("st")
    tp = lax.axis_index("tp")
    length = tokens.shape[0]
    width = tokens.shape[1]
    plen = kv_in.shape[1]
    pass_dev = store.shape[0] // plen
    blocks = length // BLK
    slots = blocks * KP
    group = q.shape[1] // HEAD
    ret_heads = rate_ref.shape[0]
    depth = n // PLANE
    my_q = lax.rem(me, PLANE)
    my_z = lax.div(me, PLANE)
    half_tok = length // 2
    half_store = store.shape[0] // 2

    pairs = (
        (store_hbm, store),
        (wk_hbm, wk),
        (wv_hbm, wv),
        (tokens_hbm, tokens),
        (wrq_hbm, wrq),
        (wrk_hbm, wrk),
        (wrv_hbm, wrv),
        (og_hbm, og),
        (wq_hbm, wq),
    )
    loads = [pltpu.make_async_copy(a, b, load_sem.at[i]) for i, (a, b) in enumerate(pairs)]
    for load in loads:
        load.start()

    barrier = pltpu.get_barrier_semaphore()

    def greet(i, carry):
        pl.semaphore_signal(
            barrier, inc=1, device_id={"st": lax.rem(me + i, n)}, device_id_type=MESH
        )
        return carry

    lax.fori_loop(1, n, greet, 0)
    pl.semaphore_signal(barrier, inc=1, device_id={"tp": 1 - tp}, device_id_type=MESH)

    for s in range(slots):
        owner_of[s] = lax.div(ids_ref[s // KP, s % KP], pass_dev)

    def invert(o, carry):
        local = jnp.int32(0)
        where = jnp.int32(0)
        for s in range(slots):
            ident = ids_ref[s // KP, s % KP]
            hit = owner_of[s] == o
            local = jnp.where(hit, lax.rem(ident, pass_dev), local)
            where = jnp.where(hit, jnp.int32(s), where)
        slot_of[o] = where
        req_out[o] = jnp.full(req_out.shape[1:], local, jnp.int32)
        return carry

    lax.fori_loop(0, n, invert, 0)

    def exchange(out_ref, in_ref, send, recv, i):
        target = lax.rem(me + i, n)
        return pltpu.make_async_remote_copy(
            src_ref=out_ref.at[target],
            dst_ref=in_ref.at[me],
            send_sem=send.at[target],
            recv_sem=recv.at[me],
            device_id={"st": target},
            device_id_type=MESH,
        )

    def arrival(out_ref, in_ref, send, recv, i):
        source = lax.rem(me + i, n)
        return pltpu.make_async_remote_copy(
            src_ref=out_ref.at[source],
            dst_ref=in_ref.at[source],
            send_sem=send.at[source],
            recv_sem=recv.at[source],
            device_id={"st": source},
            device_id_type=MESH,
        )

    def start_all(*refs):
        def body(i, carry):
            exchange(*refs, i).start()
            return carry

        lax.fori_loop(1, n, body, 0)

    def wait_recv_all(*refs):
        def body(i, carry):
            arrival(*refs, i).wait_recv()
            return carry

        lax.fori_loop(1, n, body, 0)

    def wait_send_all(*refs):
        def body(i, carry):
            exchange(*refs, i).wait_send()
            return carry

        lax.fori_loop(1, n, body, 0)

    reqs = (req_out, req_in, req_send, req_recv)
    kvs = (kv_out, kv_in, kv_send, kv_recv)
    gks = (gk_out, gk_in, gk_send, gk_recv)
    gvs = (gv_out, gv_in, gv_send, gv_recv)

    pl.semaphore_wait(barrier, n)
    start_all(*reqs)
    req_in[me] = req_out[me]

    for load in loads[:3]:
        load.wait()
    own_kv[:, :HEAD] = nn(store[...], wk[...]).astype(BF)
    own_kv[:, HEAD:] = nn(store[...], wv[...]).astype(BF)
    wait_recv_all(*reqs)

    def names(r, p, lanes):
        row = jnp.where(req_in[r][0:1, :] == p, 1.0, 0.0).astype(F32)
        return jnp.concatenate([row] * (lanes // row.shape[1]), axis=1)

    def select(r, carry):
        chosen = jnp.zeros((plen, 2 * HEAD), F32)
        for p in range(pass_dev):
            chosen = chosen + names(r, p, 2 * HEAD) * own_kv[p * plen : (p + 1) * plen, :].astype(F32)
        kv_out[r] = chosen.astype(BF)
        return carry

    lax.fori_loop(0, n, select, 0)
    kv_in[me] = kv_out[me]
    start_all(*kvs)

    span = slices.shape[3]

    def columns_of(h, quarter):
        return pl.ds(pl.multiple_of((h * PLANE + quarter) * span, span), span)

    def share_rows(h, i):
        other = lax.rem(my_q + i, PLANE)
        return pltpu.make_async_remote_copy(
            src_ref=store.at[:, columns_of(h, other)],
            dst_ref=slices.at[h, i - 1],
            send_sem=p1_send.at[h, i - 1],
            recv_sem=p1_recv.at[h, i - 1],
            device_id={"st": my_z * PLANE + other},
            device_id_type=MESH,
        )

    for h in range(HALVES):
        for i in range(1, PLANE):
            share_rows(h, i).start()

    def project(w, out):
        def body(i, carry):
            cols = pl.ds(pl.multiple_of(i * TILE, TILE), TILE)
            out[:, cols] = nn(tokens[...], w[:, cols]).astype(BF)
            return carry

        lax.fori_loop(0, w.shape[1] // TILE, body, 0)

    loads[3].wait()
    for load, w, out in ((loads[4], wrq, rq), (loads[5], wrk, rk), (loads[6], wrv, rv)):
        load.wait()
        project(w, out)
    loads[7].wait()

    ret_key = rq.shape[1] // ret_heads
    ret_value = rv.shape[1] // ret_heads
    at_t = lax.broadcasted_iota(jnp.int32, (length, length), 0)
    at_s = lax.broadcasted_iota(jnp.int32, (length, length), 1)
    distance = (at_t - at_s).astype(F32)

    def retention(j, carry):
        kc = pl.ds(pl.multiple_of(j * ret_key, ret_key), ret_key)
        vc = pl.ds(pl.multiple_of(j * ret_value, ret_value), ret_value)
        damping = jnp.where(
            distance >= 0.0, jnp.exp(-rate_ref[j] * jnp.maximum(distance, 0.0)), 0.0
        ) * ret_key ** (-0.5)
        weights = (nt(rq[:, kc], rk[:, kc]) * damping).astype(BF)
        y = nn(weights, rv[:, vc])
        r = lax.rsqrt(jnp.mean(y * y, axis=1, keepdims=True) + EPSILON)
        c = og[:, vc].astype(F32) * gain_ref[:, vc]
        inner = jnp.mean(c * y, axis=1, keepdims=True)
        gy = (r * c - r * r * r * y * inner).astype(BF)
        gw = (nt(gy, rv[:, vc]) * damping).astype(BF)
        grq[:, kc] = nn(gw, rk[:, kc]).astype(BF)
        grk[:, kc] = tn(gw, rq[:, kc]).astype(BF)
        grv[:, vc] = tn(weights, gy).astype(BF)
        return carry

    lax.fori_loop(0, ret_heads, retention, 0)
    loads[8].wait()
    project(wq, q)

    def ret_total(i, carry):
        rows = pl.ds(pl.multiple_of(i * TILE, TILE), TILE)
        total[:, rows] = (
            nt(grq[...], wrq[rows, :]) + nt(grk[...], wrk[rows, :]) + nt(grv[...], wrv[rows, :])
        )
        return carry

    lax.fori_loop(0, width // TILE, ret_total, 0)

    wait_recv_all(*kvs)
    factor = HEAD ** (-0.5)

    def attend(b, carry):
        rows = pl.ds(pl.multiple_of(b * BLK, BLK), BLK)
        read = [kv_in[owner_of[b * KP + k]] for k in range(KP)]
        keys = jnp.concatenate([x[:, :HEAD] for x in read], axis=0)
        values = jnp.concatenate([x[:, HEAD:] for x in read], axis=0)
        cols = [slice(g * HEAD, (g + 1) * HEAD) for g in range(group)]
        queries = jnp.concatenate([q[rows, c] for c in cols], axis=0)
        expo = jnp.exp(nt(queries, keys) * factor)
        probs = expo / jnp.sum(expo, axis=1, keepdims=True)
        probs_bf = probs.astype(BF)
        attn = nn(probs_bf, values)
        grad_attn = jnp.concatenate(
            [
                og[rows, c].astype(F32) * (1.0 / (1.0 + jnp.exp(-gate_ref[:, c])))
                for c in cols
            ],
            axis=0,
        )
        grad_attn_bf = grad_attn.astype(BF)
        grad_probs = nt(grad_attn_bf, values)
        delta = jnp.sum(grad_attn * attn, axis=1, keepdims=True)
        scores = (probs * (grad_probs - delta) * factor).astype(BF)
        grad_query = nn(scores, keys).astype(BF)
        for g, c in enumerate(cols):
            gq[rows, c] = grad_query[g * BLK : (g + 1) * BLK, :]
        dk = tn(scores, queries).astype(BF)
        dv = tn(probs_bf, grad_attn_bf).astype(BF)
        for k in range(KP):
            stage_k[b * KP + k] = dk[k * plen : (k + 1) * plen, :]
            stage_v[b * KP + k] = dv[k * plen : (k + 1) * plen, :]
        return carry

    lax.fori_loop(0, blocks, attend, 0)

    def place(stage, out):
        def body(o, carry):
            out[o] = stage[slot_of[o]]
            return carry

        lax.fori_loop(0, n, body, 0)

    place(stage_k, gk_out)
    place(stage_v, gv_out)
    gk_in[me] = gk_out[me]
    gv_in[me] = gv_out[me]
    start_all(*gks)
    start_all(*gvs)

    def finish_total(i, carry):
        rows = pl.ds(pl.multiple_of(i * TILE, TILE), TILE)
        gt[:, rows] = (total[:, rows] + nt(gq[...], wq[rows, :])).astype(BF)
        return carry

    lax.fori_loop(0, width // TILE, finish_total, 0)

    def to_partner(out_ref, in_ref, half, at):
        return pltpu.make_async_remote_copy(
            src_ref=out_ref.at[pl.ds(pl.multiple_of((1 - tp) * half, half), half)],
            dst_ref=in_ref,
            send_sem=tp_send.at[at],
            recv_sem=tp_recv.at[at],
            device_id={"tp": 1 - tp},
            device_id_type=MESH,
        )

    def add_own(out_ref, in_ref, half):
        own = out_ref[pl.ds(pl.multiple_of(tp * half, half), half), :]
        in_ref[...] = (own.astype(F32) + in_ref[...].astype(F32)).astype(BF)

    token_swap = to_partner(gt, gt_in, half_tok, 0)
    token_swap.start()

    def gather_sum(in_ref, out_ref):
        for p in range(pass_dev):

            def body(r, acc):
                return acc + names(r, p, HEAD) * in_ref[r].astype(F32)

            acc = lax.fori_loop(0, n, body, jnp.zeros((plen, HEAD), F32))
            out_ref[p * plen : (p + 1) * plen, :] = acc.astype(BF)

    wait_recv_all(*gks)
    gather_sum(gk_in, pk)
    def chunk(h, quarter):
        return pl.ds((h * PLANE + quarter) * depth, depth)

    def share_key(i):
        return pltpu.make_async_remote_copy(
            src_ref=pk,
            dst_ref=pk_in.at[i - 1],
            send_sem=pk_send.at[i - 1],
            recv_sem=pk_recv.at[i - 1],
            device_id={"st": my_z * PLANE + lax.rem(my_q + i, PLANE)},
            device_id_type=MESH,
        )

    def column_reduce(h, i):
        other = lax.rem(my_z + i, depth)
        return pltpu.make_async_remote_copy(
            src_ref=p1_sum.at[h, other],
            dst_ref=p2_in.at[h, i - 1],
            send_sem=p2_send.at[h, i - 1],
            recv_sem=p2_recv.at[h, i - 1],
            device_id={"st": other * PLANE + my_q},
            device_id_type=MESH,
        )

    def column_gather(h, i, source):
        at = kg.at[(h * PLANE + my_q) * depth + source]
        return pltpu.make_async_remote_copy(
            src_ref=at,
            dst_ref=at,
            send_sem=p3_send.at[h, i - 1],
            recv_sem=p3_recv.at[h, i - 1],
            device_id={"st": lax.rem(my_z + i, depth) * PLANE + my_q},
            device_id_type=MESH,
        )

    def plane_gather(h, i, source):
        at = kg.at[chunk(h, source)]
        return pltpu.make_async_remote_copy(
            src_ref=at,
            dst_ref=at,
            send_sem=p4_send.at[h, i - 1],
            recv_sem=p4_recv.at[h, i - 1],
            device_id={"st": my_z * PLANE + lax.rem(my_q + i, PLANE)},
            device_id_type=MESH,
        )

    for i in range(1, PLANE):
        share_key(i).start()
    own_terms = [tn(store[:, columns_of(h, my_q)], pk[...]) for h in range(HALVES)]

    token_swap.wait_recv()
    add_own(gt, gt_in, half_tok)
    token_out = pltpu.make_async_copy(gt_in, gt_hbm, out_sem.at[0])
    token_out.start()

    for i in range(1, PLANE):
        share_key(i).wait_recv()
        for h in range(HALVES):
            share_rows(h, i).wait_recv()
    for h in range(HALVES):
        acc = own_terms[h]
        for i in range(1, PLANE):
            acc = acc + tn(slices[h, i - 1], pk_in[i - 1])
        acc = acc.reshape(p1_sum.shape[1:])
        p1_sum[h] = acc.astype(BF)
        for i in range(1, depth):
            column_reduce(h, i).start()

    wait_recv_all(*gvs)
    gather_sum(gv_in, pv)

    def store_grad(i, carry):
        rows = pl.ds(pl.multiple_of(i * TILE, TILE), TILE)
        gs[:, rows] = (nt(pk[...], wk[rows, :]) + nt(pv[...], wv[rows, :])).astype(BF)
        return carry

    lax.fori_loop(0, width // TILE, store_grad, 0)
    store_swap = to_partner(gs, gs_in, half_store, 1)
    store_swap.start()

    for h in range(HALVES):
        for i in range(1, depth):
            column_reduce(h, i).wait_recv()
        acc = p1_sum[h, my_z].astype(F32)
        for i in range(1, depth):
            acc = acc + p2_in[h, i - 1].astype(F32)
        kg[(h * PLANE + my_q) * depth + my_z] = acc.astype(BF)
        for i in range(1, depth):
            column_gather(h, i, my_z).start()

    store_swap.wait_recv()
    add_own(gs, gs_in, half_store)
    store_out = pltpu.make_async_copy(gs_in, gs_hbm, out_sem.at[1])
    store_out.start()

    for h in range(HALVES):
        for i in range(1, depth):
            column_gather(h, i, lax.rem(my_z + depth - i, depth)).wait_recv()
        for i in range(1, PLANE):
            plane_gather(h, i, my_q).start()
    for h in range(HALVES):
        for i in range(1, PLANE):
            plane_gather(h, i, lax.rem(my_q + PLANE - i, PLANE)).wait_recv()
    weight_out = pltpu.make_async_copy(kg, gkw_hbm, out_sem.at[2])
    weight_out.start()

    wait_send_all(*reqs)
    wait_send_all(*kvs)
    wait_send_all(*gks)
    wait_send_all(*gvs)
    token_swap.wait_send()
    store_swap.wait_send()
    for h in range(HALVES):
        for i in range(1, PLANE):
            share_rows(h, i).wait_send()
            plane_gather(h, i, my_q).wait_send()
        for i in range(1, depth):
            column_reduce(h, i).wait_send()
            column_gather(h, i, my_z).wait_send()
    for i in range(1, PLANE):
        share_key(i).wait_send()
    token_out.wait()
    store_out.wait()
    weight_out.wait()


def per_device(sizes, *args):
    (tokens, store, ids, wq, wk, wv, wrq, wrk, wrv, rate, gain, gate, og) = args
    n = sizes["st"]
    pass_dev, plen, width = store.shape
    length = tokens.shape[0]
    rows = pass_dev * plen
    weight_cols = sum(w.shape[1] for w in (wq, wk, wv, wrq, wrk, wrv))
    fits = (
        sizes["tp"] == 2
        and wk.shape[1] == HEAD
        and ids.size == n
        and n % PLANE == 0
        and width % (HALVES * n) == 0
        and width % (HALVES * PLANE * 128) == 0
        and width // (HALVES * n) % 16 == 0
        and width * weight_cols + n * plen * HEAD * 12 + length * width * 12 < 24 * 2**20
    )
    if not fits:
        return per_device_plain(*args)
    depth = n // PLANE
    piece = width // (HALVES * n)

    def vm(*shape, dtype=BF):
        return pltpu.VMEM(shape, dtype)

    any_spec = pl.BlockSpec(memory_space=pl.ANY)
    smem = pl.BlockSpec(memory_space=pltpu.SMEM)
    vmem = pl.BlockSpec(memory_space=pltpu.VMEM)
    dma = pltpu.SemaphoreType.DMA
    like = [vm(*x.shape) for x in (tokens,)] + [vm(rows, width)]
    like += [vm(*x.shape) for x in (wq, wk, wv, wrq, wrk, wrv, og)]
    qs = [vm(length, w.shape[1]) for w in (wq, wrq, wrk, wrv)]
    scratch = (
        like
        + qs
        + qs
        + [
            vm(length, width, dtype=F32),
            vm(length, width),
            vm(length // 2, width),
            vm(rows, width),
            vm(rows // 2, width),
            vm(rows, 2 * HEAD),
            vm(n, 8, 128, dtype=jnp.int32),
            vm(n, 8, 128, dtype=jnp.int32),
            vm(n, plen, 2 * HEAD),
            vm(n, plen, 2 * HEAD),
        ]
        + [vm(n, plen, HEAD)] * 6
        + [
            vm(rows, HEAD),
            vm(rows, HEAD),
            vm(HALVES, PLANE - 1, rows, width // (HALVES * PLANE)),
            vm(PLANE - 1, rows, HEAD),
            vm(HALVES, depth, piece, HEAD),
            vm(HALVES, depth - 1, piece, HEAD),
            vm(HALVES * n, piece, HEAD),
            pltpu.SMEM((n,), jnp.int32),
            pltpu.SMEM((n,), jnp.int32),
            dma((9,)),
            dma((3,)),
            dma((2,)),
            dma((2,)),
        ]
        + [dma((n,))] * 8
        + [dma((HALVES, PLANE - 1))] * 2
        + [dma((PLANE - 1,))] * 2
        + [dma((HALVES, depth - 1))] * 4
        + [dma((HALVES, PLANE - 1))] * 2
    )
    grad_tokens, grad_store, grad_key = pl.pallas_call(
        functools.partial(fused_kernel, n),
        out_shape=(
            jax.ShapeDtypeStruct((length // 2, width), BF),
            jax.ShapeDtypeStruct((rows // 2, width), BF),
            jax.ShapeDtypeStruct((HALVES * n, piece, HEAD), BF),
        ),
        in_specs=[smem, smem, vmem, vmem] + [any_spec] * 9,
        out_specs=(any_spec, any_spec, any_spec),
        scratch_shapes=scratch,
        compiler_params=pltpu.CompilerParams(
            collective_id=0, has_side_effects=True, vmem_limit_bytes=60 * 2**20
        ),
    )(
        ids,
        rate,
        gain.reshape(1, -1),
        gate.reshape(1, -1),
        tokens,
        store.reshape(rows, width),
        wq,
        wk,
        wv,
        wrq,
        wrk,
        wrv,
        og,
    )
    return (
        grad_tokens,
        grad_store.reshape(pass_dev // 2, plen, width),
        grad_key.reshape(width, HEAD).astype(F32),
    )


def solution(mesh):
    return jax.shard_map(
        functools.partial(per_device, dict(mesh.shape)),
        mesh=mesh,
        in_specs=(
            P("st", None),
            P("st", None, None),
            P("st", None),
            P(None, "tp"),
            P(None, "tp"),
            P(None, "tp"),
            P(None, "tp"),
            P(None, "tp"),
            P(None, "tp"),
            P("tp"),
            P("tp"),
            P("tp"),
            P("st", "tp"),
        ),
        out_specs=(P(("st", "tp"), None), P(("st", "tp"), None, None), P(None, "tp")),
        check_vma=False,
    )
```

profile of v0, /device:TPU:0, one launch (start us, length us, event | category | flops | bytes accessed | tf_op | source)
XLA Modules:
  0.0 91.7 jit_solution(15831450202814641108)
XLA Ops:
  0.6 86.7 %shard_map.148 = (bf16[128,2048]{1,0:T(8,128)(2,1)}, bf16[128,2048]{1,0:T(8,128)(2,1)}, bf16[32,64,256]{2,1,0:T(8,128)(2,1)}) custom-call(s32[4,4]{1,0:T(4,128)} %ids_ref.1, f32[4]{0:T(128)} %rate_ref.1, f32[1,1024]{1,0:T(1,128)} %bitcast.9, f32[1,1024]{1,0:T(1,128)} %bitcast.10, bf16[256,2048]{1,0:T(8,128)(2,1)} %tokens_hbm.1, bf16[256,2048]{1,0:T(8,128)(2,1)} %bitcast.7, ...), custom_call_target="tpu_custom_call" | custom-call | tf_op jit(solution)/shard_map/pallas_call | solution.py:806
  87.3 0.0 copy-start.1
  87.3 0.0 copy-start
  87.4 2.8 %bitcast_convert_fusion = f32[2048,256]{1,0:T(8,128)} fusion(bf16[32,64,256]{2,1,0:T(8,128)(2,1)} %get-tuple-element.8), kind=kLoop, calls=%fused_computation | loop fusion | flops 524288 | bytes 3145728 | tf_op jit(solution)/shard_map/convert_element_type | solution.py:837
  90.1 0.0 copy-done.1
  90.1 0.8 copy.18
  90.9 0.0 copy-done
  90.9 0.8 copy.19
Async XLA Ops:
  87.3 2.8 %copy-start.1 = (bf16[128,2048]{1,0:T(8,128)(2,1)S(1)}, bf16[128,2048]{1,0:T(8,128)(2,1)}, u32[]{:S(2)}) copy-start(bf16[128,2048]{1,0:T(8,128)(2,1)} %get-tuple-element.12) | copy-start | bytes 1572868
  87.3 3.6 %copy-start = (bf16[128,2048]{1,0:T(8,128)(2,1)S(1)}, bf16[128,2048]{1,0:T(8,128)(2,1)}, u32[]{:S(2)}) copy-start(bf16[128,2048]{1,0:T(8,128)(2,1)} %get-tuple-element.7) | copy-start | bytes 1572868
where the time goes:
time: 91.9 us; the launch traced here: 91.7 us
  Pallas kernels  86.7 us (94%)
  other arithmetic  2.79 us (3%)
  local copies, waits for them, and re-layouts  1.59 us (2%)
    pallas_call x1, Pallas kernels, per_device(): pl.pallas_call(functools.partial(fused_kernel, n), out_shape=(jax.ShapeDt...  86.7 us
    convert_element_type x1, other arithmetic, per_device(): grad_key.reshape(width, HEAD).astype(F32)  2.79 us

commit v1 on v0

--- a/solution.py
+++ b/solution.py
@@ -216,7 +216,8 @@
 
 
 PLANE = 4
-HALVES = 2
+PARTS = 2
+SPAN = 128
 TILE = 256
 BF = jnp.bfloat16
 F32 = jnp.float32
@@ -275,11 +276,11 @@
     gt_in,
     gs,
     gs_in,
-    own_kv,
+    kv_col,
+    kv_out,
+    kv_in,
     req_out,
     req_in,
-    kv_out,
-    kv_in,
     stage_k,
     stage_v,
     gk_out,
@@ -295,20 +296,25 @@
     kg,
     owner_of,
     slot_of,
+    local_of,
     load_sem,
     out_sem,
     tp_send,
     tp_recv,
     req_send,
     req_recv,
+    gv_send,
+    gv_recv,
+    gk_send,
+    gk_recv,
+    z_send,
+    z_recv,
     kv_send,
     kv_recv,
-    gk_send,
-    gk_recv,
-    gv_send,
-    gv_recv,
-    p1_send,
-    p1_recv,
+    rows_send,
+    rows_recv,
+    swap_send,
+    swap_recv,
     pk_send,
     pk_recv,
     p2_send,
@@ -346,19 +352,27 @@
         (wq_hbm, wq),
     )
     loads = [pltpu.make_async_copy(a, b, load_sem.at[i]) for i, (a, b) in enumerate(pairs)]
-    for load in loads:
+    for load in loads[:3]:
         load.start()
 
     barrier = pltpu.get_barrier_semaphore()
-
-    def greet(i, carry):
-        pl.semaphore_signal(
-            barrier, inc=1, device_id={"st": lax.rem(me + i, n)}, device_id_type=MESH
-        )
-        return carry
-
-    lax.fori_loop(1, n, greet, 0)
-    pl.semaphore_signal(barrier, inc=1, device_id={"tp": 1 - tp}, device_id_type=MESH)
+    has_up = my_z < depth - 1
+    has_down = my_z > 0
+
+    def greet(axis, index):
+        pl.semaphore_signal(barrier, inc=1, device_id={axis: index}, device_id_type=MESH)
+
+    @pl.when(has_up)
+    def _():
+        greet("st", me + PLANE)
+
+    @pl.when(has_down)
+    def _():
+        greet("st", me - PLANE)
+
+    for i in range(1, PLANE):
+        greet("st", my_z * PLANE + lax.rem(my_q + i, PLANE))
+    greet("tp", 1 - tp)
 
     for s in range(slots):
         owner_of[s] = lax.div(ids_ref[s // KP, s % KP], pass_dev)
@@ -372,13 +386,28 @@
             local = jnp.where(hit, lax.rem(ident, pass_dev), local)
             where = jnp.where(hit, jnp.int32(s), where)
         slot_of[o] = where
-        req_out[o] = jnp.full(req_out.shape[1:], local, jnp.int32)
+        local_of[o] = local
         return carry
 
     lax.fori_loop(0, n, invert, 0)
+    row_at = lax.broadcasted_iota(jnp.int32, req_out.shape[1:], 0)
+    for c in range(PLANE):
+        tile = jnp.zeros(req_out.shape[1:], jnp.int32)
+        for z in range(depth):
+            tile = jnp.where(row_at == z, local_of[z * PLANE + c], tile)
+        req_out[c] = tile
+
+    for load in loads[3:]:
+        load.start()
+
+    def peer(i):
+        step = lax.div(i, PLANE)
+        dz = jnp.where(my_z * 2 < depth, step, lax.rem(depth - step, depth))
+        return lax.rem(my_z + dz, depth), lax.rem(my_q + lax.rem(i, PLANE), PLANE)
 
     def exchange(out_ref, in_ref, send, recv, i):
-        target = lax.rem(me + i, n)
+        z, c = peer(i)
+        target = z * PLANE + c
         return pltpu.make_async_remote_copy(
             src_ref=out_ref.at[target],
             dst_ref=in_ref.at[me],
@@ -389,7 +418,8 @@
         )
 
     def arrival(out_ref, in_ref, send, recv, i):
-        source = lax.rem(me + i, n)
+        z, c = peer(i)
+        source = z * PLANE + c
         return pltpu.make_async_remote_copy(
             src_ref=out_ref.at[source],
             dst_ref=in_ref.at[source],
@@ -399,12 +429,12 @@
             device_id_type=MESH,
         )
 
-    def start_all(*refs):
+    def start_some(lo, hi, *refs):
         def body(i, carry):
             exchange(*refs, i).start()
             return carry
 
-        lax.fori_loop(1, n, body, 0)
+        lax.fori_loop(lo, hi, body, 0)
 
     def wait_recv_all(*refs):
         def body(i, carry):
@@ -420,68 +450,182 @@
 
         lax.fori_loop(1, n, body, 0)
 
-    reqs = (req_out, req_in, req_send, req_recv)
-    kvs = (kv_out, kv_in, kv_send, kv_recv)
-    gks = (gk_out, gk_in, gk_send, gk_recv)
+    def ask(i):
+        z, c = peer(i)
+        return pltpu.make_async_remote_copy(
+            src_ref=req_out.at[c],
+            dst_ref=req_in.at[me],
+            send_sem=req_send.at[z * PLANE + c],
+            recv_sem=req_recv.at[me],
+            device_id={"st": z * PLANE + c},
+            device_id_type=MESH,
+        )
+
+    def asked(i):
+        z, c = peer(i)
+        return pltpu.make_async_remote_copy(
+            src_ref=req_out.at[c],
+            dst_ref=req_in.at[z * PLANE + c],
+            send_sem=req_send.at[z * PLANE + c],
+            recv_sem=req_recv.at[z * PLANE + c],
+            device_id={"st": z * PLANE + c},
+            device_id_type=MESH,
+        )
+
+    gks = [
+        (gk_out.at[c], gk_in.at[c], gk_send.at[c], gk_recv.at[c]) for c in range(PARTS)
+    ]
     gvs = (gv_out, gv_in, gv_send, gv_recv)
 
-    pl.semaphore_wait(barrier, n)
-    start_all(*reqs)
-    req_in[me] = req_out[me]
+    pl.semaphore_wait(
+        barrier, PLANE + has_up.astype(jnp.int32) + has_down.astype(jnp.int32)
+    )
+    for i in range(1, PLANE):
+        ask(i).start()
+    req_in[me] = req_out[my_q]
+
+    def along(up, z, p):
+        at = kv_col.at[z, pl.ds(pl.multiple_of(p * plen, plen), plen)]
+        return pltpu.make_async_remote_copy(
+            src_ref=at,
+            dst_ref=at,
+            send_sem=z_send.at[up, z, p],
+            recv_sem=z_recv.at[z, p],
+            device_id={"st": me + (2 * up - 1) * PLANE},
+            device_id_type=MESH,
+        )
 
     for load in loads[:3]:
         load.wait()
-    own_kv[:, :HEAD] = nn(store[...], wk[...]).astype(BF)
-    own_kv[:, HEAD:] = nn(store[...], wv[...]).astype(BF)
-    wait_recv_all(*reqs)
-
-    def names(r, p, lanes):
-        row = jnp.where(req_in[r][0:1, :] == p, 1.0, 0.0).astype(F32)
-        return jnp.concatenate([row] * (lanes // row.shape[1]), axis=1)
-
-    def select(r, carry):
+    kv_col[my_z, :, :HEAD] = nn(store[...], wk[...]).astype(BF)
+    kv_col[my_z, :, HEAD:] = nn(store[...], wv[...]).astype(BF)
+    for p in range(pass_dev):
+
+        @pl.when(has_up)
+        def _():
+            along(1, my_z, p).start()
+
+        @pl.when(has_down)
+        def _():
+            along(0, my_z, p).start()
+
+    def pump(k, p):
+        @pl.when(my_z - k >= 0)
+        def _():
+            along(1, my_z - k, p).wait_recv()
+
+            @pl.when(has_up)
+            def _():
+                along(1, my_z - k, p).start()
+
+        @pl.when(my_z + k < depth)
+        def _():
+            along(0, my_z + k, p).wait_recv()
+
+            @pl.when(has_down)
+            def _():
+                along(0, my_z + k, p).start()
+
+    def names(row, p, lanes):
+        mask = jnp.where(row == p, 1.0, 0.0).astype(F32)
+        return jnp.concatenate([mask] * (lanes // mask.shape[1]), axis=1)
+
+    def pick(row, z):
         chosen = jnp.zeros((plen, 2 * HEAD), F32)
         for p in range(pass_dev):
-            chosen = chosen + names(r, p, 2 * HEAD) * own_kv[p * plen : (p + 1) * plen, :].astype(F32)
-        kv_out[r] = chosen.astype(BF)
-        return carry
-
-    lax.fori_loop(0, n, select, 0)
-    kv_in[me] = kv_out[me]
-    start_all(*kvs)
-
-    span = slices.shape[3]
-
-    def columns_of(h, quarter):
-        return pl.ds(pl.multiple_of((h * PLANE + quarter) * span, span), span)
-
-    def share_rows(h, i):
+            chosen = chosen + names(row, p, 2 * HEAD) * kv_col[
+                z, p * plen : (p + 1) * plen, :
+            ].astype(F32)
+        return chosen.astype(BF)
+
+    def hand(z, i):
+        return pltpu.make_async_remote_copy(
+            src_ref=kv_out.at[z, i - 1],
+            dst_ref=kv_in.at[z * PLANE + my_q],
+            send_sem=kv_send.at[z, i - 1],
+            recv_sem=kv_recv.at[z * PLANE + my_q],
+            device_id={"st": my_z * PLANE + lax.rem(my_q + i, PLANE)},
+            device_id_type=MESH,
+        )
+
+    def handed(z, i):
+        owner = z * PLANE + lax.rem(my_q + i, PLANE)
+        return pltpu.make_async_remote_copy(
+            src_ref=kv_out.at[z, i - 1],
+            dst_ref=kv_in.at[owner],
+            send_sem=kv_send.at[z, i - 1],
+            recv_sem=kv_recv.at[owner],
+            device_id={"st": my_z * PLANE + lax.rem(my_q + i, PLANE)},
+            device_id_type=MESH,
+        )
+
+    def spread(z):
+        def body(i, carry):
+            mate = my_z * PLANE + lax.rem(my_q + i, PLANE)
+            kv_out[z, i - 1] = pick(req_in[mate, pl.ds(z, 1), :], z)
+            hand(z, i).start()
+            return carry
+
+        lax.fori_loop(1, PLANE, body, 0)
+        kv_in[z * PLANE + my_q] = pick(req_in[me, pl.ds(z, 1), :], z)
+
+    def spread_round(k):
+        def side(s, carry):
+            z = my_z + k * (2 * s - 1)
+
+            @pl.when((z >= 0) & (z < depth))
+            def _():
+                spread(z)
+
+            return carry
+
+        lax.fori_loop(0, 2, side, 0)
+
+    quarter = width // PLANE
+    share = quarter // 2
+
+    def share_rows(i):
         other = lax.rem(my_q + i, PLANE)
         return pltpu.make_async_remote_copy(
-            src_ref=store.at[:, columns_of(h, other)],
-            dst_ref=slices.at[h, i - 1],
-            send_sem=p1_send.at[h, i - 1],
-            recv_sem=p1_recv.at[h, i - 1],
+            src_ref=store.at[:, pl.ds(pl.multiple_of(other * quarter + tp * share, share), share)],
+            dst_ref=slices.at[i - 1, tp],
+            send_sem=rows_send.at[i - 1],
+            recv_sem=rows_recv.at[i - 1],
             device_id={"st": my_z * PLANE + other},
             device_id_type=MESH,
         )
 
-    for h in range(HALVES):
-        for i in range(1, PLANE):
-            share_rows(h, i).start()
-
-    def project(w, out):
+    def swap_rows(i, part):
+        return pltpu.make_async_remote_copy(
+            src_ref=slices.at[i - 1, part],
+            dst_ref=slices.at[i - 1, part],
+            send_sem=swap_send.at[i - 1],
+            recv_sem=swap_recv.at[i - 1],
+            device_id={"tp": 1 - tp},
+            device_id_type=MESH,
+        )
+
+    def project(w, out, then=None):
         def body(i, carry):
             cols = pl.ds(pl.multiple_of(i * TILE, TILE), TILE)
             out[:, cols] = nn(tokens[...], w[:, cols]).astype(BF)
+            if then is not None:
+                then(i)
             return carry
 
         lax.fori_loop(0, w.shape[1] // TILE, body, 0)
 
     loads[3].wait()
-    for load, w, out in ((loads[4], wrq, rq), (loads[5], wrk, rk), (loads[6], wrv, rv)):
+    for load, w, out in ((loads[4], wrq, rq), (loads[5], wrk, rk)):
         load.wait()
         project(w, out)
+    for i in range(1, PLANE):
+        asked(i).wait_recv()
+    spread(my_z)
+    for i in range(1, PLANE):
+        share_rows(i).start()
+    loads[6].wait()
+    project(wrv, rv)
     loads[7].wait()
 
     ret_key = rq.shape[1] // ret_heads
@@ -489,6 +633,11 @@
     at_t = lax.broadcasted_iota(jnp.int32, (length, length), 0)
     at_s = lax.broadcasted_iota(jnp.int32, (length, length), 1)
     distance = (at_t - at_s).astype(F32)
+
+    def pump_part(k, i, count):
+        each = pass_dev // count
+        for p in range(each):
+            pump(k, i * each + p)
 
     def retention(j, carry):
         kc = pl.ds(pl.multiple_of(j * ret_key, ret_key), ret_key)
@@ -506,22 +655,42 @@
         grq[:, kc] = nn(gw, rk[:, kc]).astype(BF)
         grk[:, kc] = tn(gw, rq[:, kc]).astype(BF)
         grv[:, vc] = tn(weights, gy).astype(BF)
+        pump_part(1, j, ret_heads)
         return carry
 
     lax.fori_loop(0, ret_heads, retention, 0)
+    spread_round(1)
     loads[8].wait()
-    project(wq, q)
+    project(wq, q, lambda i: pump_part(2, i, wq.shape[1] // TILE))
+    spread_round(2)
 
     def ret_total(i, carry):
-        rows = pl.ds(pl.multiple_of(i * TILE, TILE), TILE)
+        wide = width // pass_dev
+        rows = pl.ds(pl.multiple_of(i * wide, wide), wide)
         total[:, rows] = (
             nt(grq[...], wrq[rows, :]) + nt(grk[...], wrk[rows, :]) + nt(grv[...], wrv[rows, :])
         )
+        pump_part(3, i, pass_dev)
         return carry
 
-    lax.fori_loop(0, width // TILE, ret_total, 0)
-
-    wait_recv_all(*kvs)
+    lax.fori_loop(0, pass_dev, ret_total, 0)
+    spread_round(3)
+    for i in range(1, PLANE):
+        share_rows(i).wait_recv()
+        swap_rows(i, tp).start()
+
+    def wait_handed(z, carry):
+        for i in range(1, PLANE):
+            handed(z, i).wait_recv()
+        return carry
+
+    lax.fori_loop(0, depth, wait_handed, 0)
+
+    def ask_far(i, carry):
+        ask(i).start()
+        return carry
+
+    lax.fori_loop(PLANE, n, ask_far, 0)
     factor = HEAD ** (-0.5)
 
     def attend(b, carry):
@@ -552,7 +721,8 @@
         dk = tn(scores, queries).astype(BF)
         dv = tn(probs_bf, grad_attn_bf).astype(BF)
         for k in range(KP):
-            stage_k[b * KP + k] = dk[k * plen : (k + 1) * plen, :]
+            for c in range(PARTS):
+                stage_k[c, b * KP + k] = dk[k * plen : (k + 1) * plen, c * SPAN : (c + 1) * SPAN]
             stage_v[b * KP + k] = dv[k * plen : (k + 1) * plen, :]
         return carry
 
@@ -565,12 +735,13 @@
 
         lax.fori_loop(0, n, body, 0)
 
-    place(stage_k, gk_out)
+    for c in range(PARTS):
+        place(stage_k.at[c], gk_out.at[c])
+        start_some(1, n, *gks[c])
     place(stage_v, gv_out)
-    gk_in[me] = gk_out[me]
+    for c in range(PARTS):
+        gk_in[c, me] = gk_out[c, me]
     gv_in[me] = gv_out[me]
-    start_all(*gks)
-    start_all(*gvs)
 
     def finish_total(i, carry):
         rows = pl.ds(pl.multiple_of(i * TILE, TILE), TILE)
@@ -597,140 +768,202 @@
     token_swap.start()
 
     def gather_sum(in_ref, out_ref):
+        lanes = out_ref.shape[1]
         for p in range(pass_dev):
 
             def body(r, acc):
-                return acc + names(r, p, HEAD) * in_ref[r].astype(F32)
-
-            acc = lax.fori_loop(0, n, body, jnp.zeros((plen, HEAD), F32))
+                row = req_in[r, pl.ds(my_z, 1), :]
+                return acc + names(row, p, lanes) * in_ref[r].astype(F32)
+
+            acc = lax.fori_loop(0, n, body, jnp.zeros((plen, lanes), F32))
             out_ref[p * plen : (p + 1) * plen, :] = acc.astype(BF)
 
-    wait_recv_all(*gks)
-    gather_sum(gk_in, pk)
-    def chunk(h, quarter):
-        return pl.ds((h * PLANE + quarter) * depth, depth)
-
-    def share_key(i):
-        return pltpu.make_async_remote_copy(
-            src_ref=pk,
-            dst_ref=pk_in.at[i - 1],
-            send_sem=pk_send.at[i - 1],
-            recv_sem=pk_recv.at[i - 1],
+    def share_key(c, i):
+        return pltpu.make_async_remote_copy(
+            src_ref=pk.at[c],
+            dst_ref=pk_in.at[c, i - 1],
+            send_sem=pk_send.at[c, i - 1],
+            recv_sem=pk_recv.at[c, i - 1],
             device_id={"st": my_z * PLANE + lax.rem(my_q + i, PLANE)},
             device_id_type=MESH,
         )
 
-    def column_reduce(h, i):
+    def column_reduce(c, i):
         other = lax.rem(my_z + i, depth)
         return pltpu.make_async_remote_copy(
-            src_ref=p1_sum.at[h, other],
-            dst_ref=p2_in.at[h, i - 1],
-            send_sem=p2_send.at[h, i - 1],
-            recv_sem=p2_recv.at[h, i - 1],
+            src_ref=p1_sum.at[c, other],
+            dst_ref=p2_in.at[c, i - 1],
+            send_sem=p2_send.at[c, i - 1],
+            recv_sem=p2_recv.at[c, i - 1],
             device_id={"st": other * PLANE + my_q},
             device_id_type=MESH,
         )
 
-    def column_gather(h, i, source):
-        at = kg.at[(h * PLANE + my_q) * depth + source]
+    def column_gather(c, i, source):
+        at = kg.at[c, my_q * depth + source]
         return pltpu.make_async_remote_copy(
             src_ref=at,
             dst_ref=at,
-            send_sem=p3_send.at[h, i - 1],
-            recv_sem=p3_recv.at[h, i - 1],
+            send_sem=p3_send.at[c, i - 1],
+            recv_sem=p3_recv.at[c, i - 1],
             device_id={"st": lax.rem(my_z + i, depth) * PLANE + my_q},
             device_id_type=MESH,
         )
 
-    def plane_gather(h, i, source):
-        at = kg.at[chunk(h, source)]
+    def plane_gather(c, i, source, z):
+        at = kg.at[c, source * depth + z]
         return pltpu.make_async_remote_copy(
             src_ref=at,
             dst_ref=at,
-            send_sem=p4_send.at[h, i - 1],
-            recv_sem=p4_recv.at[h, i - 1],
+            send_sem=p4_send.at[c, z, i - 1],
+            recv_sem=p4_recv.at[c, z, i - 1],
             device_id={"st": my_z * PLANE + lax.rem(my_q + i, PLANE)},
             device_id_type=MESH,
         )
 
     for i in range(1, PLANE):
-        share_key(i).start()
-    own_terms = [tn(store[:, columns_of(h, my_q)], pk[...]) for h in range(HALVES)]
+        swap_rows(i, 1 - tp).wait_recv()
+
+    def asked_far(i, carry):
+        asked(i).wait_recv()
+        return carry
+
+    lax.fori_loop(PLANE, n, asked_far, 0)
+
+    own_cols = pl.ds(pl.multiple_of(my_q * quarter, quarter), quarter)
+    own_terms = []
+    for c in range(PARTS):
+        wait_recv_all(*gks[c])
+        gather_sum(gk_in.at[c], pk.at[c])
+        for i in range(1, PLANE):
+            share_key(c, i).start()
+        own_terms.append(tn(store[:, own_cols], pk[c]))
+        if c == 0:
+            start_some(PLANE, 2 * PLANE, *gvs)
 
     token_swap.wait_recv()
     add_own(gt, gt_in, half_tok)
     token_out = pltpu.make_async_copy(gt_in, gt_hbm, out_sem.at[0])
     token_out.start()
 
-    for i in range(1, PLANE):
-        share_key(i).wait_recv()
-        for h in range(HALVES):
-            share_rows(h, i).wait_recv()
-    for h in range(HALVES):
-        acc = own_terms[h]
+    for c in range(PARTS):
         for i in range(1, PLANE):
-            acc = acc + tn(slices[h, i - 1], pk_in[i - 1])
-        acc = acc.reshape(p1_sum.shape[1:])
-        p1_sum[h] = acc.astype(BF)
+            share_key(c, i).wait_recv()
+        for part in range(2):
+            acc = own_terms[c][part * share : (part + 1) * share]
+            for i in range(1, PLANE):
+                acc = acc + tn(slices[i - 1, part], pk_in[c, i - 1])
+            acc = acc.reshape(depth // 2, -1, SPAN)
+            p1_sum[c, part * depth // 2 : (part + 1) * depth // 2] = acc.astype(BF)
         for i in range(1, depth):
-            column_reduce(h, i).start()
+            column_reduce(c, i).start()
+        start_some((c + 2) * PLANE, (c + 3) * PLANE, *gvs)
+
+    for c in range(PARTS):
+        for i in range(1, depth):
+            column_reduce(c, i).wait_recv()
+        acc = p1_sum[c, my_z].astype(F32)
+        for i in range(1, depth):
+            acc = acc + p2_in[c, i - 1].astype(F32)
+        kg[c, my_q * depth + my_z] = acc.astype(BF)
+        for i in range(1, depth):
+            column_gather(c, i, my_z).start()
+        for i in range(1, PLANE):
+            plane_gather(c, i, my_q, my_z).start()
+    start_some(1, PLANE, *gvs)
+
+    for c in range(PARTS):
+        for s in range(1, depth):
+            i = jnp.where(my_z * 2 < depth, depth - s, s)
+            source = lax.rem(my_z + depth - i, depth)
+            column_gather(c, i, source).wait_recv()
+            for j in range(1, PLANE):
+                plane_gather(c, j, my_q, source).start()
 
     wait_recv_all(*gvs)
     gather_sum(gv_in, pv)
 
     def store_grad(i, carry):
         rows = pl.ds(pl.multiple_of(i * TILE, TILE), TILE)
-        gs[:, rows] = (nt(pk[...], wk[rows, :]) + nt(pv[...], wv[rows, :])).astype(BF)
+        keys = jnp.concatenate([pk[c] for c in range(PARTS)], axis=1)
+        gs[:, rows] = (nt(keys, wk[rows, :]) + nt(pv[...], wv[rows, :])).astype(BF)
         return carry
 
     lax.fori_loop(0, width // TILE, store_grad, 0)
     store_swap = to_partner(gs, gs_in, half_store, 1)
     store_swap.start()
-
-    for h in range(HALVES):
-        for i in range(1, depth):
-            column_reduce(h, i).wait_recv()
-        acc = p1_sum[h, my_z].astype(F32)
-        for i in range(1, depth):
-            acc = acc + p2_in[h, i - 1].astype(F32)
-        kg[(h * PLANE + my_q) * depth + my_z] = acc.astype(BF)
-        for i in range(1, depth):
-            column_gather(h, i, my_z).start()
-
     store_swap.wait_recv()
     add_own(gs, gs_in, half_store)
     store_out = pltpu.make_async_copy(gs_in, gs_hbm, out_sem.at[1])
     store_out.start()
 
-    for h in range(HALVES):
-        for i in range(1, depth):
-            column_gather(h, i, lax.rem(my_z + depth - i, depth)).wait_recv()
-        for i in range(1, PLANE):
-            plane_gather(h, i, my_q).start()
-    for h in range(HALVES):
-        for i in range(1, PLANE):
-            plane_gather(h, i, lax.rem(my_q + PLANE - i, PLANE)).wait_recv()
+    for c in range(PARTS):
+        for z in range(depth):
+            for i in range(1, PLANE):
+                plane_gather(c, i, lax.rem(my_q + PLANE - i, PLANE), z).wait_recv()
     weight_out = pltpu.make_async_copy(kg, gkw_hbm, out_sem.at[2])
     weight_out.start()
 
-    wait_send_all(*reqs)
-    wait_send_all(*kvs)
-    wait_send_all(*gks)
+    def ask_done(i, carry):
+        ask(i).wait_send()
+        return carry
+
+    lax.fori_loop(1, n, ask_done, 0)
+
+    def along_done(z, carry):
+        for p in range(pass_dev):
+
+            @pl.when(has_up & (z <= my_z))
+            def _():
+                along(1, z, p).wait_send()
+
+            @pl.when(has_down & (z >= my_z))
+            def _():
+                along(0, z, p).wait_send()
+
+        for i in range(1, PLANE):
+            hand(z, i).wait_send()
+        return carry
+
+    lax.fori_loop(0, depth, along_done, 0)
     wait_send_all(*gvs)
     token_swap.wait_send()
     store_swap.wait_send()
-    for h in range(HALVES):
+    for c in range(PARTS):
+        wait_send_all(*gks[c])
         for i in range(1, PLANE):
-            share_rows(h, i).wait_send()
-            plane_gather(h, i, my_q).wait_send()
+            share_key(c, i).wait_send()
+            for z in range(depth):
+                plane_gather(c, i, my_q, z).wait_send()
         for i in range(1, depth):
-            column_reduce(h, i).wait_send()
-            column_gather(h, i, my_z).wait_send()
+            column_reduce(c, i).wait_send()
+            column_gather(c, i, my_z).wait_send()
     for i in range(1, PLANE):
-        share_key(i).wait_send()
+        share_rows(i).wait_send()
+        swap_rows(i, tp).wait_send()
     token_out.wait()
     store_out.wait()
     weight_out.wait()
+
+
+def finish_kernel(gt_hbm, gs_hbm, kg_hbm, ot_hbm, os_hbm, ok_hbm, gt, gs, kg, out, in_sem, out_sem):
+    loads = [
+        pltpu.make_async_copy(a, b, in_sem.at[i])
+        for i, (a, b) in enumerate(((kg_hbm.at[0], kg.at[0]), (kg_hbm.at[1], kg.at[1]), (gt_hbm, gt), (gs_hbm, gs)))
+    ]
+    for load in loads:
+        load.start()
+    for c in range(PARTS):
+        loads[c].wait()
+        out[:, c * SPAN : (c + 1) * SPAN] = kg[c].astype(F32)
+    stores = [pltpu.make_async_copy(out, ok_hbm, out_sem.at[0])]
+    stores[0].start()
+    for i, (a, b) in enumerate(((gt, ot_hbm), (gs, os_hbm))):
+        loads[2 + i].wait()
+        stores.append(pltpu.make_async_copy(a, b, out_sem.at[1 + i]))
+        stores[-1].start()
+    for store in stores:
+        store.wait()
 
 
 def per_device(sizes, *args):
@@ -743,17 +976,19 @@
     fits = (
         sizes["tp"] == 2
         and wk.shape[1] == HEAD
+        and HEAD == PARTS * SPAN
         and ids.size == n
-        and n % PLANE == 0
-        and width % (HALVES * n) == 0
-        and width % (HALVES * PLANE * 128) == 0
-        and width // (HALVES * n) % 16 == 0
+        and n == PLANE * 4
+        and pass_dev == 4
+        and rate.shape[0] == 4
+        and wq.shape[1] == 4 * TILE
+        and width % (n * 128) == 0
         and width * weight_cols + n * plen * HEAD * 12 + length * width * 12 < 24 * 2**20
     )
     if not fits:
         return per_device_plain(*args)
     depth = n // PLANE
-    piece = width // (HALVES * n)
+    piece = width // n
 
     def vm(*shape, dtype=BF):
         return pltpu.VMEM(shape, dtype)
@@ -775,21 +1010,25 @@
             vm(length // 2, width),
             vm(rows, width),
             vm(rows // 2, width),
-            vm(rows, 2 * HEAD),
+            vm(depth, rows, 2 * HEAD),
+            vm(depth, PLANE - 1, plen, 2 * HEAD),
+            vm(n, plen, 2 * HEAD),
+            vm(PLANE, 8, 128, dtype=jnp.int32),
             vm(n, 8, 128, dtype=jnp.int32),
-            vm(n, 8, 128, dtype=jnp.int32),
-            vm(n, plen, 2 * HEAD),
-            vm(n, plen, 2 * HEAD),
-        ]
-        + [vm(n, plen, HEAD)] * 6
-        + [
+            vm(PARTS, n, plen, SPAN),
+            vm(n, plen, HEAD),
+            vm(PARTS, n, plen, SPAN),
+            vm(n, plen, HEAD),
+            vm(PARTS, n, plen, SPAN),
+            vm(n, plen, HEAD),
+            vm(PARTS, rows, SPAN),
             vm(rows, HEAD),
-            vm(rows, HEAD),
-            vm(HALVES, PLANE - 1, rows, width // (HALVES * PLANE)),
-            vm(PLANE - 1, rows, HEAD),
-            vm(HALVES, depth, piece, HEAD),
-            vm(HALVES, depth - 1, piece, HEAD),
-            vm(HALVES * n, piece, HEAD),
+            vm(PLANE - 1, 2, rows, width // (2 * PLANE)),
+            vm(PARTS, PLANE - 1, rows, SPAN),
+            vm(PARTS, depth, piece, SPAN),
+            vm(PARTS, depth - 1, piece, SPAN),
+            vm(PARTS, n, piece, SPAN),
+            pltpu.SMEM((n,), jnp.int32),
             pltpu.SMEM((n,), jnp.int32),
             pltpu.SMEM((n,), jnp.int32),
             dma((9,)),
@@ -797,18 +1036,21 @@
             dma((2,)),
             dma((2,)),
         ]
-        + [dma((n,))] * 8
-        + [dma((HALVES, PLANE - 1))] * 2
-        + [dma((PLANE - 1,))] * 2
-        + [dma((HALVES, depth - 1))] * 4
-        + [dma((HALVES, PLANE - 1))] * 2
+        + [dma((n,))] * 4
+        + [dma((PARTS, n))] * 2
+        + [dma((2, depth, pass_dev)), dma((depth, pass_dev))]
+        + [dma((depth, PLANE - 1)), dma((n,))]
+        + [dma((PLANE - 1,))] * 4
+        + [dma((PARTS, PLANE - 1))] * 2
+        + [dma((PARTS, depth - 1))] * 4
+        + [dma((PARTS, depth, PLANE - 1))] * 2
     )
     grad_tokens, grad_store, grad_key = pl.pallas_call(
         functools.partial(fused_kernel, n),
         out_shape=(
             jax.ShapeDtypeStruct((length // 2, width), BF),
             jax.ShapeDtypeStruct((rows // 2, width), BF),
-            jax.ShapeDtypeStruct((HALVES * n, piece, HEAD), BF),
+            jax.ShapeDtypeStruct((PARTS, n, piece, SPAN), BF),
         ),
         in_specs=[smem, smem, vmem, vmem] + [any_spec] * 9,
         out_specs=(any_spec, any_spec, any_spec),
@@ -831,11 +1073,25 @@
         wrv,
         og,
     )
-    return (
-        grad_tokens,
-        grad_store.reshape(pass_dev // 2, plen, width),
-        grad_key.reshape(width, HEAD).astype(F32),
-    )
+    grad_tokens, grad_store, grad_key = pl.pallas_call(
+        finish_kernel,
+        out_shape=(
+            jax.ShapeDtypeStruct((length // 2, width), BF),
+            jax.ShapeDtypeStruct((rows // 2, width), BF),
+            jax.ShapeDtypeStruct((width, HEAD), F32),
+        ),
+        in_specs=[any_spec] * 3,
+        out_specs=(any_spec, any_spec, any_spec),
+        scratch_shapes=[
+            vm(length // 2, width),
+            vm(rows // 2, width),
+            vm(PARTS, width, SPAN),
+            vm(width, HEAD, dtype=F32),
+            dma((4,)),
+            dma((3,)),
+        ],
+    )(grad_tokens, grad_store, grad_key.reshape(PARTS, width, SPAN))
+    return (grad_tokens, grad_store.reshape(pass_dev // 2, plen, width), grad_key)
 
 
 def solution(mesh):

time: 91.9 us -> 81.8 us (0.89)
  Pallas kernels: 86.7 us -> 80.8 us
  other arithmetic: 2.79 us -> 0 us
  local copies, waits for them, and re-layouts: 1.59 us -> 0 us
    pallas_call x1, Pallas kernels: 86.7 us -> 77.8 us  [per_device(): pl.pallas_call(functools.partial(fused_kernel, n), out_shape=(jax.ShapeDt...]
    pallas_call x0 -> x1, Pallas kernels: none -> 2.99 us  [per_device(): pl.pallas_call(finish_kernel, out_shape=(jax.ShapeDtypeStruct((length //...]
    convert_element_type x1 -> x0, other arithmetic: 2.79 us -> none  [per_device(): grad_key.reshape(width, HEAD).astype(F32)]
    unnamed x6 -> x0, local copies, waits for them, and re-layouts: 1.59 us -> none
where the time goes in v1:
time: 81.8 us; the launch traced here: 81.4 us
  Pallas kernels  80.8 us (99%)
    pallas_call x1, Pallas kernels, per_device(): pl.pallas_call(functools.partial(fused_kernel, n), out_shape=(jax.ShapeDt...  77.8 us
    pallas_call x1, Pallas kernels, per_device(): pl.pallas_call(finish_kernel, out_shape=(jax.ShapeDtypeStruct((length //...  2.99 us

profile of v1, /device:TPU:0, one launch (start us, length us, event | category | flops | bytes accessed | tf_op | source)
XLA Modules:
  0.0 81.4 jit_solution(15441562350529911032)
XLA Ops:
  0.6 77.8 %shard_map.148 = (bf16[128,2048]{1,0:T(8,128)(2,1)}, bf16[128,2048]{1,0:T(8,128)(2,1)}, bf16[2,16,128,128]{3,2,1,0:T(8,128)(2,1)}) custom-call(s32[4,4]{1,0:T(4,128)} %ids_ref.1, f32[4]{0:T(128)} %rate_ref.1, f32[1,1024]{1,0:T(1,128)} %bitcast.7, f32[1,1024]{1,0:T(1,128)} %bitcast.8, bf16[256,2048]{1,0:T(8,128)(2,1)} %tokens_hbm.1, ...), custom_call_target="tpu_custom_call" | custom-call | tf_op jit(solution)/shard_map/pallas_call | solution.py:1048
  78.4 3.0 %shard_map.149 = (bf16[128,2048]{1,0:T(8,128)(2,1)}, bf16[128,2048]{1,0:T(8,128)(2,1)}, f32[2048,256]{1,0:T(8,128)}) custom-call(bf16[128,2048]{1,0:T(8,128)(2,1)} %get-tuple-element.9.gt_hbm, bf16[128,2048]{1,0:T(8,128)(2,1)} %get-tuple-element.10.gs_hbm, bf16[2,2048,128]{2,1,0:T(8,128)(2,1)} %bitcast.6), custom_call_target="tpu_custom_call" | custom-call | tf_op jit(solution)/shard_map/pallas_call | solution.py:1076

commit v2 on v1

--- a/solution.py
+++ b/solution.py
@@ -218,6 +218,9 @@
 PLANE = 4
 PARTS = 2
 SPAN = 128
+CHUNKS = 4
+SWAPS = 4
+TOGETHER = 2
 TILE = 256
 BF = jnp.bfloat16
 F32 = jnp.float32
@@ -274,8 +277,11 @@
     total,
     gt,
     gt_in,
+    gs_key,
     gs,
     gs_in,
+    ga,
+    ga_bf,
     kv_col,
     kv_out,
     kv_in,
@@ -286,7 +292,10 @@
     gk_out,
     gv_out,
     gk_in,
-    gv_in,
+    v_in,
+    vp_out,
+    v_mid,
+    v_add,
     pk,
     pv,
     slices,
@@ -303,8 +312,10 @@
     tp_recv,
     req_send,
     req_recv,
-    gv_send,
-    gv_recv,
+    v_send,
+    v_recv,
+    vp_send,
+    vp_recv,
     gk_send,
     gk_recv,
     z_send,
@@ -411,23 +422,24 @@
         return pltpu.make_async_remote_copy(
             src_ref=out_ref.at[target],
             dst_ref=in_ref.at[me],
-            send_sem=send.at[target],
-            recv_sem=recv.at[me],
+            send_sem=send,
+            recv_sem=recv,
             device_id={"st": target},
             device_id_type=MESH,
         )
 
-    def arrival(out_ref, in_ref, send, recv, i):
-        z, c = peer(i)
-        source = z * PLANE + c
-        return pltpu.make_async_remote_copy(
-            src_ref=out_ref.at[source],
-            dst_ref=in_ref.at[source],
-            send_sem=send.at[source],
-            recv_sem=recv.at[source],
-            device_id={"st": source},
-            device_id_type=MESH,
-        )
+    def bulk(ref, send, recv):
+        return pltpu.make_async_remote_copy(
+            src_ref=ref,
+            dst_ref=ref,
+            send_sem=send,
+            recv_sem=recv,
+            device_id={"tp": 1 - tp},
+            device_id_type=MESH,
+        )
+
+    def bulk_all(out_ref, in_ref, send, recv):
+        return bulk(in_ref.at[pl.ds(0, n - 1)], send, recv)
 
     def start_some(lo, hi, *refs):
         def body(i, carry):
@@ -436,60 +448,41 @@
 
         lax.fori_loop(lo, hi, body, 0)
 
-    def wait_recv_all(*refs):
-        def body(i, carry):
-            arrival(*refs, i).wait_recv()
-            return carry
-
-        lax.fori_loop(1, n, body, 0)
-
-    def wait_send_all(*refs):
-        def body(i, carry):
-            exchange(*refs, i).wait_send()
-            return carry
-
-        lax.fori_loop(1, n, body, 0)
-
-    def ask(i):
+    def ask(i, far):
         z, c = peer(i)
         return pltpu.make_async_remote_copy(
             src_ref=req_out.at[c],
             dst_ref=req_in.at[me],
-            send_sem=req_send.at[z * PLANE + c],
-            recv_sem=req_recv.at[me],
+            send_sem=req_send.at[far],
+            recv_sem=req_recv.at[far],
             device_id={"st": z * PLANE + c},
             device_id_type=MESH,
         )
 
-    def asked(i):
-        z, c = peer(i)
-        return pltpu.make_async_remote_copy(
-            src_ref=req_out.at[c],
-            dst_ref=req_in.at[z * PLANE + c],
-            send_sem=req_send.at[z * PLANE + c],
-            recv_sem=req_recv.at[z * PLANE + c],
-            device_id={"st": z * PLANE + c},
-            device_id_type=MESH,
-        )
-
+    asked_near = bulk(req_in.at[pl.ds(0, PLANE - 1)], req_send.at[0], req_recv.at[0])
+    asked_far = bulk(req_in.at[pl.ds(0, n - PLANE)], req_send.at[1], req_recv.at[1])
     gks = [
         (gk_out.at[c], gk_in.at[c], gk_send.at[c], gk_recv.at[c]) for c in range(PARTS)
     ]
-    gvs = (gv_out, gv_in, gv_send, gv_recv)
 
     pl.semaphore_wait(
         barrier, PLANE + has_up.astype(jnp.int32) + has_down.astype(jnp.int32)
     )
     for i in range(1, PLANE):
-        ask(i).start()
+        ask(i, 0).start()
     req_in[me] = req_out[my_q]
 
+    grain = plen // CHUNKS
+
+    def grain_of(p):
+        return pl.ds(pl.multiple_of(p * grain, grain), grain)
+
     def along(up, z, p):
-        at = kv_col.at[z, pl.ds(pl.multiple_of(p * plen, plen), plen)]
+        at = kv_col.at[z, :, grain_of(p)]
         return pltpu.make_async_remote_copy(
             src_ref=at,
             dst_ref=at,
-            send_sem=z_send.at[up, z, p],
+            send_sem=z_send.at[up, z],
             recv_sem=z_recv.at[z, p],
             device_id={"st": me + (2 * up - 1) * PLANE},
             device_id_type=MESH,
@@ -497,9 +490,10 @@
 
     for load in loads[:3]:
         load.wait()
-    kv_col[my_z, :, :HEAD] = nn(store[...], wk[...]).astype(BF)
-    kv_col[my_z, :, HEAD:] = nn(store[...], wv[...]).astype(BF)
-    for p in range(pass_dev):
+    own_shape = (pass_dev, plen, HEAD)
+    kv_col[my_z, :, :, :HEAD] = nn(store[...], wk[...]).astype(BF).reshape(own_shape)
+    kv_col[my_z, :, :, HEAD:] = nn(store[...], wv[...]).astype(BF).reshape(own_shape)
+    for p in range(CHUNKS):
 
         @pl.when(has_up)
         def _():
@@ -509,73 +503,49 @@
         def _():
             along(0, my_z, p).start()
 
-    def pump(k, p):
-        @pl.when(my_z - k >= 0)
-        def _():
-            along(1, my_z - k, p).wait_recv()
-
-            @pl.when(has_up)
-            def _():
-                along(1, my_z - k, p).start()
-
-        @pl.when(my_z + k < depth)
-        def _():
-            along(0, my_z + k, p).wait_recv()
-
-            @pl.when(has_down)
-            def _():
-                along(0, my_z + k, p).start()
-
     def names(row, p, lanes):
         mask = jnp.where(row == p, 1.0, 0.0).astype(F32)
         return jnp.concatenate([mask] * (lanes // mask.shape[1]), axis=1)
 
-    def pick(row, z):
-        chosen = jnp.zeros((plen, 2 * HEAD), F32)
-        for p in range(pass_dev):
-            chosen = chosen + names(row, p, 2 * HEAD) * kv_col[
-                z, p * plen : (p + 1) * plen, :
-            ].astype(F32)
-        return chosen.astype(BF)
-
-    def hand(z, i):
-        return pltpu.make_async_remote_copy(
-            src_ref=kv_out.at[z, i - 1],
-            dst_ref=kv_in.at[z * PLANE + my_q],
-            send_sem=kv_send.at[z, i - 1],
-            recv_sem=kv_recv.at[z * PLANE + my_q],
+    def hand(z, p, i):
+        return pltpu.make_async_remote_copy(
+            src_ref=kv_out.at[z, i - 1, grain_of(p)],
+            dst_ref=kv_in.at[z * PLANE + my_q, grain_of(p)],
+            send_sem=kv_send.at[0],
+            recv_sem=kv_recv.at[0],
             device_id={"st": my_z * PLANE + lax.rem(my_q + i, PLANE)},
             device_id_type=MESH,
         )
 
-    def handed(z, i):
-        owner = z * PLANE + lax.rem(my_q + i, PLANE)
-        return pltpu.make_async_remote_copy(
-            src_ref=kv_out.at[z, i - 1],
-            dst_ref=kv_in.at[owner],
-            send_sem=kv_send.at[z, i - 1],
-            recv_sem=kv_recv.at[owner],
-            device_id={"st": my_z * PLANE + lax.rem(my_q + i, PLANE)},
-            device_id_type=MESH,
-        )
-
-    def spread(z):
-        def body(i, carry):
-            mate = my_z * PLANE + lax.rem(my_q + i, PLANE)
-            kv_out[z, i - 1] = pick(req_in[mate, pl.ds(z, 1), :], z)
-            hand(z, i).start()
-            return carry
-
-        lax.fori_loop(1, PLANE, body, 0)
-        kv_in[z * PLANE + my_q] = pick(req_in[me, pl.ds(z, 1), :], z)
-
-    def spread_round(k):
-        def side(s, carry):
-            z = my_z + k * (2 * s - 1)
+    def spread(z, p):
+        rows = [kv_col[z, k, grain_of(p), :].astype(F32) for k in range(pass_dev)]
+
+        def pick(reader):
+            row = req_in[my_z * PLANE + reader, pl.ds(z, 1), :]
+            chosen = names(row, 0, 2 * HEAD) * rows[0]
+            for k in range(1, pass_dev):
+                chosen = chosen + names(row, k, 2 * HEAD) * rows[k]
+            return chosen.astype(BF)
+
+        for i in range(1, PLANE):
+            kv_out[z, i - 1, grain_of(p), :] = pick(lax.rem(my_q + i, PLANE))
+        kv_in[z * PLANE + my_q, grain_of(p), :] = pick(my_q)
+        for i in range(1, PLANE):
+            hand(z, p, i).start()
+
+    def pump(k, p):
+        def side(up, carry):
+            z = my_z + k * (1 - 2 * up)
 
             @pl.when((z >= 0) & (z < depth))
             def _():
-                spread(z)
+                along(up, z, p).wait_recv()
+
+                @pl.when(jnp.where(up == 1, has_up, has_down))
+                def _():
+                    along(up, z, p).start()
+
+                spread(z, p)
 
             return carry
 
@@ -588,22 +558,16 @@
         other = lax.rem(my_q + i, PLANE)
         return pltpu.make_async_remote_copy(
             src_ref=store.at[:, pl.ds(pl.multiple_of(other * quarter + tp * share, share), share)],
-            dst_ref=slices.at[i - 1, tp],
-            send_sem=rows_send.at[i - 1],
-            recv_sem=rows_recv.at[i - 1],
+            dst_ref=slices.at[tp, i - 1],
+            send_sem=rows_send.at[0],
+            recv_sem=rows_recv.at[0],
             device_id={"st": my_z * PLANE + other},
             device_id_type=MESH,
         )
 
-    def swap_rows(i, part):
-        return pltpu.make_async_remote_copy(
-            src_ref=slices.at[i - 1, part],
-            dst_ref=slices.at[i - 1, part],
-            send_sem=swap_send.at[i - 1],
-            recv_sem=swap_recv.at[i - 1],
-            device_id={"tp": 1 - tp},
-            device_id_type=MESH,
-        )
+    rows_shared = bulk(slices.at[tp], rows_send.at[0], rows_recv.at[0])
+    rows_swap = bulk(slices.at[tp], swap_send.at[0], swap_recv.at[0])
+    rows_swapped = bulk(slices.at[1 - tp], swap_send.at[0], swap_recv.at[0])
 
     def project(w, out, then=None):
         def body(i, carry):
@@ -619,9 +583,13 @@
     for load, w, out in ((loads[4], wrq, rq), (loads[5], wrk, rk)):
         load.wait()
         project(w, out)
-    for i in range(1, PLANE):
-        asked(i).wait_recv()
-    spread(my_z)
+    asked_near.wait_recv()
+
+    def spread_own(p, carry):
+        spread(my_z, p)
+        return carry
+
+    lax.fori_loop(0, CHUNKS, spread_own, 0)
     for i in range(1, PLANE):
         share_rows(i).start()
     loads[6].wait()
@@ -633,11 +601,6 @@
     at_t = lax.broadcasted_iota(jnp.int32, (length, length), 0)
     at_s = lax.broadcasted_iota(jnp.int32, (length, length), 1)
     distance = (at_t - at_s).astype(F32)
-
-    def pump_part(k, i, count):
-        each = pass_dev // count
-        for p in range(each):
-            pump(k, i * each + p)
 
     def retention(j, carry):
         kc = pl.ds(pl.multiple_of(j * ret_key, ret_key), ret_key)
@@ -655,78 +618,79 @@
         grq[:, kc] = nn(gw, rk[:, kc]).astype(BF)
         grk[:, kc] = tn(gw, rq[:, kc]).astype(BF)
         grv[:, vc] = tn(weights, gy).astype(BF)
-        pump_part(1, j, ret_heads)
+        pump(1, j)
         return carry
 
     lax.fori_loop(0, ret_heads, retention, 0)
-    spread_round(1)
     loads[8].wait()
-    project(wq, q, lambda i: pump_part(2, i, wq.shape[1] // TILE))
-    spread_round(2)
+    project(wq, q, lambda i: pump(2, i))
 
     def ret_total(i, carry):
-        wide = width // pass_dev
+        wide = width // CHUNKS
         rows = pl.ds(pl.multiple_of(i * wide, wide), wide)
         total[:, rows] = (
             nt(grq[...], wrq[rows, :]) + nt(grk[...], wrk[rows, :]) + nt(grv[...], wrv[rows, :])
         )
-        pump_part(3, i, pass_dev)
+        pump(3, i)
         return carry
 
-    lax.fori_loop(0, pass_dev, ret_total, 0)
-    spread_round(3)
-    for i in range(1, PLANE):
-        share_rows(i).wait_recv()
-        swap_rows(i, tp).start()
-
-    def wait_handed(z, carry):
-        for i in range(1, PLANE):
-            handed(z, i).wait_recv()
+    lax.fori_loop(0, CHUNKS, ret_total, 0)
+    rows_shared.wait_recv()
+    rows_swap.start()
+    cols = [slice(g * HEAD, (g + 1) * HEAD) for g in range(group)]
+    gate = 1.0 / (1.0 + jnp.exp(-gate_ref[...]))
+
+    def gated(b, carry):
+        rows = pl.ds(pl.multiple_of(b * BLK, BLK), BLK)
+        for g, c in enumerate(cols):
+            at = slice(g * BLK, (g + 1) * BLK)
+            grad_attn = og[rows, c].astype(F32) * gate[:, c]
+            ga[b, at, :] = grad_attn
+            ga_bf[b, at, :] = grad_attn.astype(BF)
         return carry
 
-    lax.fori_loop(0, depth, wait_handed, 0)
+    lax.fori_loop(0, blocks, gated, 0)
+    bulk(kv_in.at[pl.ds(0, n - depth)], kv_send.at[0], kv_recv.at[0]).wait_recv()
 
     def ask_far(i, carry):
-        ask(i).start()
+        ask(i, 1).start()
         return carry
 
     lax.fori_loop(PLANE, n, ask_far, 0)
     factor = HEAD ** (-0.5)
 
-    def attend(b, carry):
-        rows = pl.ds(pl.multiple_of(b * BLK, BLK), BLK)
-        read = [kv_in[owner_of[b * KP + k]] for k in range(KP)]
-        keys = jnp.concatenate([x[:, :HEAD] for x in read], axis=0)
-        values = jnp.concatenate([x[:, HEAD:] for x in read], axis=0)
-        cols = [slice(g * HEAD, (g + 1) * HEAD) for g in range(group)]
-        queries = jnp.concatenate([q[rows, c] for c in cols], axis=0)
-        expo = jnp.exp(nt(queries, keys) * factor)
-        probs = expo / jnp.sum(expo, axis=1, keepdims=True)
-        probs_bf = probs.astype(BF)
-        attn = nn(probs_bf, values)
-        grad_attn = jnp.concatenate(
-            [
-                og[rows, c].astype(F32) * (1.0 / (1.0 + jnp.exp(-gate_ref[:, c])))
-                for c in cols
-            ],
-            axis=0,
-        )
-        grad_attn_bf = grad_attn.astype(BF)
-        grad_probs = nt(grad_attn_bf, values)
-        delta = jnp.sum(grad_attn * attn, axis=1, keepdims=True)
-        scores = (probs * (grad_probs - delta) * factor).astype(BF)
-        grad_query = nn(scores, keys).astype(BF)
-        for g, c in enumerate(cols):
-            gq[rows, c] = grad_query[g * BLK : (g + 1) * BLK, :]
-        dk = tn(scores, queries).astype(BF)
-        dv = tn(probs_bf, grad_attn_bf).astype(BF)
-        for k in range(KP):
-            for c in range(PARTS):
-                stage_k[c, b * KP + k] = dk[k * plen : (k + 1) * plen, c * SPAN : (c + 1) * SPAN]
-            stage_v[b * KP + k] = dv[k * plen : (k + 1) * plen, :]
+    def attend(step, carry):
+        group_of = [step * TOGETHER + t for t in range(TOGETHER)]
+        rows = [pl.ds(pl.multiple_of(b * BLK, BLK), BLK) for b in group_of]
+        read = [[kv_in[owner_of[b * KP + k]] for k in range(KP)] for b in group_of]
+        keys = [jnp.concatenate([x[:, :HEAD] for x in each], axis=0) for each in read]
+        values = [jnp.concatenate([x[:, HEAD:] for x in each], axis=0) for each in read]
+        queries = [jnp.concatenate([q[r, c] for c in cols], axis=0) for r in rows]
+        expo = [jnp.exp(nt(a, b) * factor) for a, b in zip(queries, keys)]
+        grad_probs = [nt(ga_bf[b], v) for b, v in zip(group_of, values)]
+        probs = [e / jnp.sum(e, axis=1, keepdims=True) for e in expo]
+        probs_bf = [x.astype(BF) for x in probs]
+        attn = [nn(x, v) for x, v in zip(probs_bf, values)]
+        delta = [
+            jnp.sum(ga[b] * a, axis=1, keepdims=True) for b, a in zip(group_of, attn)
+        ]
+        scores = [
+            (x * (g - d) * factor).astype(BF) for x, g, d in zip(probs, grad_probs, delta)
+        ]
+        dk = [tn(x, a).astype(BF) for x, a in zip(scores, queries)]
+        dv = [tn(x, ga_bf[b]).astype(BF) for x, b in zip(probs_bf, group_of)]
+        grad_query = [nn(x, a).astype(BF) for x, a in zip(scores, keys)]
+        for t, b in enumerate(group_of):
+            for g, c in enumerate(cols):
+                gq[rows[t], c] = grad_query[t][g * BLK : (g + 1) * BLK, :]
+            for k in range(KP):
+                at = slice(k * plen, (k + 1) * plen)
+                for c in range(PARTS):
+                    stage_k[c, b * KP + k] = dk[t][at, c * SPAN : (c + 1) * SPAN]
+                stage_v[b * KP + k] = dv[t][at, :]
         return carry
 
-    lax.fori_loop(0, blocks, attend, 0)
+    lax.fori_loop(0, blocks // TOGETHER, attend, 0)
 
     def place(stage, out):
         def body(o, carry):
@@ -735,13 +699,32 @@
 
         lax.fori_loop(0, n, body, 0)
 
-    for c in range(PARTS):
-        place(stage_k.at[c], gk_out.at[c])
-        start_some(1, n, *gks[c])
+    is_end = (my_z == 0) | (my_z == depth - 1)
+    upper = my_z * 2 >= depth
+    near_end = jnp.where(upper, depth - 1, 0)
+    near_mid = jnp.where(upper, depth - 2, 1)
+    far_end = depth - 1 - near_end
+    far_mid = depth - 1 - near_mid
+
+    def hand_value(z, i, part):
+        mate = lax.rem(my_q + i, PLANE)
+        return pltpu.make_async_remote_copy(
+            src_ref=gv_out.at[z * PLANE + mate],
+            dst_ref=v_in.at[z, my_q],
+            send_sem=v_send.at[part],
+            recv_sem=v_recv.at[part],
+            device_id={"st": my_z * PLANE + mate},
+            device_id_type=MESH,
+        )
+
+    place(stage_k.at[0], gk_out.at[0])
+    start_some(1, n, *gks[0])
+    place(stage_k.at[1], gk_out.at[1])
     place(stage_v, gv_out)
     for c in range(PARTS):
         gk_in[c, me] = gk_out[c, me]
-    gv_in[me] = gv_out[me]
+    for z in range(depth):
+        v_in[z, my_q] = gv_out[z * PLANE + my_q]
 
     def finish_total(i, carry):
         rows = pl.ds(pl.multiple_of(i * TILE, TILE), TILE)
@@ -749,6 +732,9 @@
         return carry
 
     lax.fori_loop(0, width // TILE, finish_total, 0)
+    for z in (far_end, far_mid):
+        for i in range(1, PLANE):
+            hand_value(z, i, 0).start()
 
     def to_partner(out_ref, in_ref, half, at):
         return pltpu.make_async_remote_copy(
@@ -769,21 +755,22 @@
 
     def gather_sum(in_ref, out_ref):
         lanes = out_ref.shape[1]
-        for p in range(pass_dev):
-
-            def body(r, acc):
-                row = req_in[r, pl.ds(my_z, 1), :]
-                return acc + names(row, p, lanes) * in_ref[r].astype(F32)
-
-            acc = lax.fori_loop(0, n, body, jnp.zeros((plen, lanes), F32))
-            out_ref[p * plen : (p + 1) * plen, :] = acc.astype(BF)
+
+        def body(r, sums):
+            row = req_in[r, pl.ds(my_z, 1), :]
+            term = in_ref[r].astype(F32)
+            return tuple(s + names(row, p, lanes) * term for p, s in enumerate(sums))
+
+        sums = lax.fori_loop(0, n, body, (jnp.zeros((plen, lanes), F32),) * pass_dev)
+        for p, s in enumerate(sums):
+            out_ref[p * plen : (p + 1) * plen, :] = s.astype(BF)
 
     def share_key(c, i):
         return pltpu.make_async_remote_copy(
             src_ref=pk.at[c],
             dst_ref=pk_in.at[c, i - 1],
-            send_sem=pk_send.at[c, i - 1],
-            recv_sem=pk_recv.at[c, i - 1],
+            send_sem=pk_send.at[c],
+            recv_sem=pk_recv.at[c],
             device_id={"st": my_z * PLANE + lax.rem(my_q + i, PLANE)},
             device_id_type=MESH,
         )
@@ -793,53 +780,98 @@
         return pltpu.make_async_remote_copy(
             src_ref=p1_sum.at[c, other],
             dst_ref=p2_in.at[c, i - 1],
-            send_sem=p2_send.at[c, i - 1],
-            recv_sem=p2_recv.at[c, i - 1],
+            send_sem=p2_send.at[c],
+            recv_sem=p2_recv.at[c],
             device_id={"st": other * PLANE + my_q},
             device_id_type=MESH,
         )
 
-    def column_gather(c, i, source):
-        at = kg.at[c, my_q * depth + source]
+    def column_gather(c, up, z):
+        at = kg.at[c, my_q * depth + z]
         return pltpu.make_async_remote_copy(
             src_ref=at,
             dst_ref=at,
-            send_sem=p3_send.at[c, i - 1],
-            recv_sem=p3_recv.at[c, i - 1],
-            device_id={"st": lax.rem(my_z + i, depth) * PLANE + my_q},
-            device_id_type=MESH,
-        )
-
-    def plane_gather(c, i, source, z):
-        at = kg.at[c, source * depth + z]
+            send_sem=p3_send.at[up, c],
+            recv_sem=p3_recv.at[c, z],
+            device_id={"st": me + (2 * up - 1) * PLANE},
+            device_id_type=MESH,
+        )
+
+    def plane_gather(c, i, z):
+        at = kg.at[c, my_q * depth + z]
         return pltpu.make_async_remote_copy(
             src_ref=at,
             dst_ref=at,
-            send_sem=p4_send.at[c, z, i - 1],
-            recv_sem=p4_recv.at[c, z, i - 1],
+            send_sem=p4_send.at[c],
+            recv_sem=p4_recv.at[c],
             device_id={"st": my_z * PLANE + lax.rem(my_q + i, PLANE)},
             device_id_type=MESH,
         )
 
-    for i in range(1, PLANE):
-        swap_rows(i, 1 - tp).wait_recv()
-
-    def asked_far(i, carry):
-        asked(i).wait_recv()
-        return carry
-
-    lax.fori_loop(PLANE, n, asked_far, 0)
+    def send_part(at, dst, sem, z):
+        return pltpu.make_async_remote_copy(
+            src_ref=vp_out.at[at],
+            dst_ref=dst,
+            send_sem=vp_send.at[0],
+            recv_sem=vp_recv.at[sem],
+            device_id={"st": z * PLANE + my_q},
+            device_id_type=MESH,
+        )
+
+    def merge(z, out_ref, *more):
+        def body(p, carry):
+            at = pl.ds(pl.multiple_of(p * plen, plen), plen)
+            acc = jnp.zeros((plen, HEAD), F32)
+            for r in range(PLANE):
+                row = req_in[my_z * PLANE + r, pl.ds(z, 1), :]
+                acc = acc + names(row, p, HEAD) * v_in[z, r].astype(F32)
+            for ref in more:
+                acc = acc + ref[at, :].astype(F32)
+            out_ref[at, :] = acc.astype(BF)
+            return carry
+
+        lax.fori_loop(0, pass_dev, body, 0)
+
+    def pass_near():
+        z = jnp.where(is_end, near_mid, near_end)
+        merge(z, vp_out.at[2])
+        send_part(2, v_add.at[0], 2, z).start()
+
+    def pass_first(which):
+        z = (far_mid, far_end)[which]
+
+        @pl.when(is_end)
+        def _():
+            merge(z, vp_out.at[which])
+            send_part(which, v_mid.at[which], which, near_mid).start()
+
+    def pass_second(which):
+        z = (far_mid, far_end)[which]
+
+        @pl.when(jnp.logical_not(is_end))
+        def _():
+            bulk(v_mid.at[which], vp_send.at[0], vp_recv.at[which]).wait_recv()
+            merge(z, vp_out.at[which], v_mid.at[which])
+            send_part(which, v_add.at[1], 3, z).start()
+
+    rows_swapped.wait_recv()
+    asked_far.wait_recv()
 
     own_cols = pl.ds(pl.multiple_of(my_q * quarter, quarter), quarter)
     own_terms = []
     for c in range(PARTS):
-        wait_recv_all(*gks[c])
+        bulk_all(*gks[c]).wait_recv()
+        if c == 0:
+            start_some(1, n, *gks[1])
         gather_sum(gk_in.at[c], pk.at[c])
         for i in range(1, PLANE):
             share_key(c, i).start()
         own_terms.append(tn(store[:, own_cols], pk[c]))
         if c == 0:
-            start_some(PLANE, 2 * PLANE, *gvs)
+            for z in (near_mid, near_end):
+                for i in range(1, PLANE):
+                    hand_value(z, i, 1).start()
+    v_half = [bulk(gv_out.at[pl.ds(0, 2 * (PLANE - 1))], v_send.at[h], v_recv.at[h]) for h in range(2)]
 
     token_swap.wait_recv()
     add_own(gt, gt_in, half_tok)
@@ -847,120 +879,186 @@
     token_out.start()
 
     for c in range(PARTS):
-        for i in range(1, PLANE):
-            share_key(c, i).wait_recv()
+        bulk(pk_in.at[c], pk_send.at[c], pk_recv.at[c]).wait_recv()
         for part in range(2):
             acc = own_terms[c][part * share : (part + 1) * share]
             for i in range(1, PLANE):
-                acc = acc + tn(slices[i - 1, part], pk_in[c, i - 1])
+                acc = acc + tn(slices[part, i - 1], pk_in[c, i - 1])
             acc = acc.reshape(depth // 2, -1, SPAN)
             p1_sum[c, part * depth // 2 : (part + 1) * depth // 2] = acc.astype(BF)
         for i in range(1, depth):
             column_reduce(c, i).start()
-        start_some((c + 2) * PLANE, (c + 3) * PLANE, *gvs)
+        if c == 0:
+            v_half[0].wait_recv()
+            pass_first(0)
+
+    def key_store_grad(i, carry):
+        rows = pl.ds(pl.multiple_of(i * TILE, TILE), TILE)
+        keys = jnp.concatenate([pk[c] for c in range(PARTS)], axis=1)
+        gs_key[:, rows] = nt(keys, wk[rows, :])
+        return carry
+
+    lax.fori_loop(0, width // TILE, key_store_grad, 0)
 
     for c in range(PARTS):
-        for i in range(1, depth):
-            column_reduce(c, i).wait_recv()
+        bulk(p2_in.at[c], p2_send.at[c], p2_recv.at[c]).wait_recv()
         acc = p1_sum[c, my_z].astype(F32)
         for i in range(1, depth):
             acc = acc + p2_in[c, i - 1].astype(F32)
         kg[c, my_q * depth + my_z] = acc.astype(BF)
-        for i in range(1, depth):
-            column_gather(c, i, my_z).start()
+
+        @pl.when(has_up)
+        def _():
+            column_gather(c, 1, my_z).start()
+
+        @pl.when(has_down)
+        def _():
+            column_gather(c, 0, my_z).start()
+
         for i in range(1, PLANE):
-            plane_gather(c, i, my_q, my_z).start()
-    start_some(1, PLANE, *gvs)
-
-    for c in range(PARTS):
-        for s in range(1, depth):
-            i = jnp.where(my_z * 2 < depth, depth - s, s)
-            source = lax.rem(my_z + depth - i, depth)
-            column_gather(c, i, source).wait_recv()
-            for j in range(1, PLANE):
-                plane_gather(c, j, my_q, source).start()
-
-    wait_recv_all(*gvs)
-    gather_sum(gv_in, pv)
+            plane_gather(c, i, my_z).start()
+        if c == 0:
+            pass_first(1)
+            pass_second(0)
+
+    v_half[1].wait_recv()
+    pass_near()
+
+    def relay(step, carry):
+        k = 1 + lax.div(step, 2 * PARTS)
+        c = lax.rem(lax.div(step, 2), PARTS)
+        up = lax.rem(step, 2)
+        z = my_z + k * (1 - 2 * up)
+
+        @pl.when((z >= 0) & (z < depth))
+        def _():
+            column_gather(c, up, z).wait_recv()
+
+            @pl.when(jnp.where(up == 1, has_up, has_down))
+            def _():
+                column_gather(c, up, z).start()
+
+            for i in range(1, PLANE):
+                plane_gather(c, i, z).start()
+
+        return carry
+
+    lax.fori_loop(0, 2 * PARTS, relay, 0)
+    pass_second(1)
+    lax.fori_loop(2 * PARTS, 2 * PARTS * (depth - 1), relay, 0)
+
+    for sem in range(2):
+        bulk(v_add.at[sem], vp_send.at[0], vp_recv.at[2 + sem]).wait_recv()
+    merge(my_z, pv, v_add.at[0], v_add.at[1])
+    wide = width // SWAPS
+
+    def cut(i):
+        return pl.ds(pl.multiple_of(i * wide, wide), wide)
+
+    def half_of(which):
+        return pl.ds(pl.multiple_of(which * half_store, half_store), half_store)
+
+    def store_swap(i):
+        return pltpu.make_async_remote_copy(
+            src_ref=gs.at[half_of(1 - tp), cut(i)],
+            dst_ref=gs_in.at[:, cut(i)],
+            send_sem=tp_send.at[1 + i],
+            recv_sem=tp_recv.at[1 + i],
+            device_id={"tp": 1 - tp},
+            device_id_type=MESH,
+        )
 
     def store_grad(i, carry):
-        rows = pl.ds(pl.multiple_of(i * TILE, TILE), TILE)
-        keys = jnp.concatenate([pk[c] for c in range(PARTS)], axis=1)
-        gs[:, rows] = (nt(keys, wk[rows, :]) + nt(pv[...], wv[rows, :])).astype(BF)
+        gs[:, cut(i)] = (gs_key[:, cut(i)] + nt(pv[...], wv[cut(i), :])).astype(BF)
+        store_swap(i).start()
         return carry
 
-    lax.fori_loop(0, width // TILE, store_grad, 0)
-    store_swap = to_partner(gs, gs_in, half_store, 1)
-    store_swap.start()
-    store_swap.wait_recv()
-    add_own(gs, gs_in, half_store)
+    lax.fori_loop(0, SWAPS, store_grad, 0)
+
+    def store_sum(i, carry):
+        store_swap(i).wait_recv()
+        own = gs[half_of(tp), cut(i)]
+        gs_in[:, cut(i)] = (own.astype(F32) + gs_in[:, cut(i)].astype(F32)).astype(BF)
+        return carry
+
+    lax.fori_loop(0, SWAPS, store_sum, 0)
     store_out = pltpu.make_async_copy(gs_in, gs_hbm, out_sem.at[1])
     store_out.start()
 
+    weight_out = []
     for c in range(PARTS):
-        for z in range(depth):
-            for i in range(1, PLANE):
-                plane_gather(c, i, lax.rem(my_q + PLANE - i, PLANE), z).wait_recv()
-    weight_out = pltpu.make_async_copy(kg, gkw_hbm, out_sem.at[2])
-    weight_out.start()
-
-    def ask_done(i, carry):
-        ask(i).wait_send()
-        return carry
-
-    lax.fori_loop(1, n, ask_done, 0)
-
-    def along_done(z, carry):
-        for p in range(pass_dev):
-
-            @pl.when(has_up & (z <= my_z))
-            def _():
-                along(1, z, p).wait_send()
-
-            @pl.when(has_down & (z >= my_z))
-            def _():
-                along(0, z, p).wait_send()
-
-        for i in range(1, PLANE):
-            hand(z, i).wait_send()
-        return carry
-
-    lax.fori_loop(0, depth, along_done, 0)
-    wait_send_all(*gvs)
+        bulk(kg.at[c, pl.ds(0, n - depth)], p4_send.at[c], p4_recv.at[c]).wait_recv()
+        weight_out.append(pltpu.make_async_copy(kg.at[c], gkw_hbm.at[c], out_sem.at[2 + c]))
+        weight_out[c].start()
+
+    asked_near.wait_send()
+    asked_far.wait_send()
+    for z in range(depth):
+
+        @pl.when(has_up & (z <= my_z))
+        def _():
+            bulk(kv_col.at[z], z_send.at[1, z], z_recv.at[z, 0]).wait_send()
+
+        @pl.when(has_down & (z >= my_z))
+        def _():
+            bulk(kv_col.at[z], z_send.at[0, z], z_recv.at[z, 0]).wait_send()
+
+    bulk(kv_out, kv_send.at[0], kv_recv.at[0]).wait_send()
+    for half in v_half:
+        half.wait_send()
+    bulk(vp_out, vp_send.at[0], vp_recv.at[0]).wait_send()
     token_swap.wait_send()
-    store_swap.wait_send()
+    for i in range(SWAPS):
+        store_swap(i).wait_send()
     for c in range(PARTS):
-        wait_send_all(*gks[c])
-        for i in range(1, PLANE):
-            share_key(c, i).wait_send()
-            for z in range(depth):
-                plane_gather(c, i, my_q, z).wait_send()
-        for i in range(1, depth):
-            column_reduce(c, i).wait_send()
-            column_gather(c, i, my_z).wait_send()
-    for i in range(1, PLANE):
-        share_rows(i).wait_send()
-        swap_rows(i, tp).wait_send()
+        bulk_all(*gks[c]).wait_send()
+        bulk(pk_in.at[c], pk_send.at[c], pk_recv.at[c]).wait_send()
+        bulk(kg.at[c, pl.ds(0, n - depth)], p4_send.at[c], p4_recv.at[c]).wait_send()
+        bulk(p2_in.at[c], p2_send.at[c], p2_recv.at[c]).wait_send()
+    for z in range(depth):
+
+        @pl.when(my_z == z)
+        def _():
+            for c in range(PARTS):
+                if z < depth - 1:
+                    at = kg.at[c, pl.ds(0, z + 1)]
+                    bulk(at, p3_send.at[1, c], p3_recv.at[c, 0]).wait_send()
+                if z > 0:
+                    at = kg.at[c, pl.ds(0, depth - z)]
+                    bulk(at, p3_send.at[0, c], p3_recv.at[c, 0]).wait_send()
+
+    rows_shared.wait_send()
+    rows_swap.wait_send()
     token_out.wait()
     store_out.wait()
-    weight_out.wait()
+    for out in weight_out:
+        out.wait()
 
 
 def finish_kernel(gt_hbm, gs_hbm, kg_hbm, ot_hbm, os_hbm, ok_hbm, gt, gs, kg, out, in_sem, out_sem):
+    pieces = in_sem.shape[0] - 2
+    span = out.shape[0] // pieces
+    cuts = [pl.ds(i * span, span) for i in range(pieces)]
     loads = [
-        pltpu.make_async_copy(a, b, in_sem.at[i])
-        for i, (a, b) in enumerate(((kg_hbm.at[0], kg.at[0]), (kg_hbm.at[1], kg.at[1]), (gt_hbm, gt), (gs_hbm, gs)))
+        pltpu.make_async_copy(kg_hbm.at[:, at], kg.at[:, at], in_sem.at[i])
+        for i, at in enumerate(cuts)
+    ]
+    loads += [
+        pltpu.make_async_copy(gt_hbm, gt, in_sem.at[pieces]),
+        pltpu.make_async_copy(gs_hbm, gs, in_sem.at[pieces + 1]),
     ]
     for load in loads:
         load.start()
-    for c in range(PARTS):
-        loads[c].wait()
-        out[:, c * SPAN : (c + 1) * SPAN] = kg[c].astype(F32)
-    stores = [pltpu.make_async_copy(out, ok_hbm, out_sem.at[0])]
-    stores[0].start()
+    stores = []
+    for i, at in enumerate(cuts):
+        loads[i].wait()
+        for c in range(PARTS):
+            out[at, c * SPAN : (c + 1) * SPAN] = kg[c, at, :].astype(F32)
+        stores.append(pltpu.make_async_copy(out.at[at], ok_hbm.at[at], out_sem.at[i]))
+        stores[-1].start()
     for i, (a, b) in enumerate(((gt, ot_hbm), (gs, os_hbm))):
-        loads[2 + i].wait()
-        stores.append(pltpu.make_async_copy(a, b, out_sem.at[1 + i]))
+        loads[pieces + i].wait()
+        stores.append(pltpu.make_async_copy(a, b, out_sem.at[pieces + i]))
         stores[-1].start()
     for store in stores:
         store.wait()
@@ -979,9 +1077,10 @@
         and HEAD == PARTS * SPAN
         and ids.size == n
         and n == PLANE * 4
-        and pass_dev == 4
-        and rate.shape[0] == 4
-        and wq.shape[1] == 4 * TILE
+        and plen % (16 * CHUNKS) == 0
+        and length % (BLK * TOGETHER) == 0
+        and rate.shape[0] == CHUNKS
+        and wq.shape[1] == CHUNKS * TILE
         and width % (n * 128) == 0
         and width * weight_cols + n * plen * HEAD * 12 + length * width * 12 < 24 * 2**20
     )
@@ -1008,9 +1107,12 @@
             vm(length, width, dtype=F32),
             vm(length, width),
             vm(length // 2, width),
+            vm(rows, width, dtype=F32),
             vm(rows, width),
             vm(rows // 2, width),
-            vm(depth, rows, 2 * HEAD),
+            vm(length // BLK, BLK * wq.shape[1] // HEAD, HEAD, dtype=F32),
+            vm(length // BLK, BLK * wq.shape[1] // HEAD, HEAD),
+            vm(depth, pass_dev, plen, 2 * HEAD),
             vm(depth, PLANE - 1, plen, 2 * HEAD),
             vm(n, plen, 2 * HEAD),
             vm(PLANE, 8, 128, dtype=jnp.int32),
@@ -1020,10 +1122,13 @@
             vm(PARTS, n, plen, SPAN),
             vm(n, plen, HEAD),
             vm(PARTS, n, plen, SPAN),
-            vm(n, plen, HEAD),
+            vm(depth, PLANE, plen, HEAD),
+            vm(3, rows, HEAD),
+            vm(2, rows, HEAD),
+            vm(2, rows, HEAD),
             vm(PARTS, rows, SPAN),
             vm(rows, HEAD),
-            vm(PLANE - 1, 2, rows, width // (2 * PLANE)),
+            vm(2, PLANE - 1, rows, width // (2 * PLANE)),
             vm(PARTS, PLANE - 1, rows, SPAN),
             vm(PARTS, depth, piece, SPAN),
             vm(PARTS, depth - 1, piece, SPAN),
@@ -1032,18 +1137,18 @@
             pltpu.SMEM((n,), jnp.int32),
             pltpu.SMEM((n,), jnp.int32),
             dma((9,)),
-            dma((3,)),
-            dma((2,)),
-            dma((2,)),
+            dma((2 + PARTS,)),
         ]
-        + [dma((n,))] * 4
-        + [dma((PARTS, n))] * 2
-        + [dma((2, depth, pass_dev)), dma((depth, pass_dev))]
-        + [dma((depth, PLANE - 1)), dma((n,))]
-        + [dma((PLANE - 1,))] * 4
-        + [dma((PARTS, PLANE - 1))] * 2
-        + [dma((PARTS, depth - 1))] * 4
-        + [dma((PARTS, depth, PLANE - 1))] * 2
+        + [dma((1 + SWAPS,))] * 2
+        + [dma((2,))] * 2
+        + [dma((2,))] * 2
+        + [dma((1,)), dma((4,))]
+        + [dma((PARTS,))] * 2
+        + [dma((2, depth)), dma((depth, CHUNKS))]
+        + [dma((1,))] * 6
+        + [dma((PARTS,))] * 4
+        + [dma((2, PARTS)), dma((PARTS, depth))]
+        + [dma((PARTS,))] * 2
     )
     grad_tokens, grad_store, grad_key = pl.pallas_call(
         functools.partial(fused_kernel, n),
@@ -1087,8 +1192,8 @@
             vm(rows // 2, width),
             vm(PARTS, width, SPAN),
             vm(width, HEAD, dtype=F32),
-            dma((4,)),
-            dma((3,)),
+            dma((6,)),
+            dma((6,)),
         ],
     )(grad_tokens, grad_store, grad_key.reshape(PARTS, width, SPAN))
     return (grad_tokens, grad_store.reshape(pass_dev // 2, plen, width), grad_key)

time: 81.8 us -> 73.9 us (0.903)
  Pallas kernels: 80.8 us -> 73 us
    pallas_call x1, Pallas kernels: 77.8 us -> 70.3 us  [per_device(): pl.pallas_call(functools.partial(fused_kernel, n), out_shape=(jax.ShapeDt...]
where the time goes in v2:
time: 73.9 us; the launch traced here: 73.7 us
  Pallas kernels  73 us (99%)
    pallas_call x1, Pallas kernels, per_device(): pl.pallas_call(functools.partial(fused_kernel, n), out_shape=(jax.ShapeDt...  70.3 us
    pallas_call x1, Pallas kernels, per_device(): pl.pallas_call(finish_kernel, out_shape=(jax.ShapeDtypeStruct((length //...  2.75 us

profile of v2, /device:TPU:0, one launch (start us, length us, event | category | flops | bytes accessed | tf_op | source)
XLA Modules:
  0.0 73.7 jit_solution(11804206156012314483)
XLA Ops:
  0.6 70.3 %shard_map.148 = (bf16[128,2048]{1,0:T(8,128)(2,1)}, bf16[128,2048]{1,0:T(8,128)(2,1)}, bf16[2,16,128,128]{3,2,1,0:T(8,128)(2,1)}) custom-call(s32[4,4]{1,0:T(4,128)} %ids_ref.1, f32[4]{0:T(128)} %rate_ref.1, f32[1,1024]{1,0:T(1,128)} %bitcast.7, f32[1,1024]{1,0:T(1,128)} %bitcast.8, bf16[256,2048]{1,0:T(8,128)(2,1)} %tokens_hbm.1, ...), custom_call_target="tpu_custom_call" | custom-call | tf_op jit(solution)/shard_map/pallas_call | solution.py:1153
  70.9 2.7 %shard_map.149 = (bf16[128,2048]{1,0:T(8,128)(2,1)}, bf16[128,2048]{1,0:T(8,128)(2,1)}, f32[2048,256]{1,0:T(8,128)}) custom-call(bf16[128,2048]{1,0:T(8,128)(2,1)} %get-tuple-element.9.gt_hbm, bf16[128,2048]{1,0:T(8,128)(2,1)} %get-tuple-element.10.gs_hbm, bf16[2,2048,128]{2,1,0:T(8,128)(2,1)} %bitcast.6), custom_call_target="tpu_custom_call" | custom-call | tf_op jit(solution)/shard_map/pallas_call | solution.py:1181

commit v3 on v2

--- a/solution.py
+++ b/solution.py
@@ -220,7 +220,8 @@
 SPAN = 128
 CHUNKS = 4
 SWAPS = 4
-TOGETHER = 2
+TOGETHER = 4
+VMEM_BYTES = 67043328
 TILE = 256
 BF = jnp.bfloat16
 F32 = jnp.float32
@@ -241,10 +242,10 @@
 
 def fused_kernel(
     n,
-    ids_ref,
-    rate_ref,
-    gain_ref,
-    gate_ref,
+    ids_hbm,
+    rate_hbm,
+    gain_hbm,
+    gate_hbm,
     tokens_hbm,
     store_hbm,
     wq_hbm,
@@ -254,9 +255,13 @@
     wrk_hbm,
     wrv_hbm,
     og_hbm,
-    gt_hbm,
-    gs_hbm,
-    gkw_hbm,
+    gt_res,
+    gs_res,
+    gkw_res,
+    ids_ref,
+    rate_ref,
+    gain_ref,
+    gate_ref,
     tokens,
     store,
     wq,
@@ -307,7 +312,7 @@
     slot_of,
     local_of,
     load_sem,
-    out_sem,
+    small_sem,
     tp_send,
     tp_recv,
     req_send,
@@ -316,6 +321,7 @@
     v_recv,
     vp_send,
     vp_recv,
+    vm_recv,
     gk_send,
     gk_recv,
     z_send,
@@ -363,7 +369,19 @@
         (wq_hbm, wq),
     )
     loads = [pltpu.make_async_copy(a, b, load_sem.at[i]) for i, (a, b) in enumerate(pairs)]
-    for load in loads[:3]:
+    small = [
+        pltpu.make_async_copy(a, b, small_sem.at[i])
+        for i, (a, b) in enumerate(
+            (
+                (ids_hbm, ids_ref),
+                (rate_hbm, rate_ref),
+                (gain_hbm, gain_ref),
+                (gate_hbm, gate_ref),
+            )
+        )
+    ]
+    small[0].start()
+    for load in loads[:3] + small[1:]:
         load.start()
 
     barrier = pltpu.get_barrier_semaphore()
@@ -385,6 +403,7 @@
         greet("st", my_z * PLANE + lax.rem(my_q + i, PLANE))
     greet("tp", 1 - tp)
 
+    small[0].wait()
     for s in range(slots):
         owner_of[s] = lax.div(ids_ref[s // KP, s % KP], pass_dev)
 
@@ -595,6 +614,8 @@
     loads[6].wait()
     project(wrv, rv)
     loads[7].wait()
+    for load in small[1:]:
+        load.wait()
 
     ret_key = rq.shape[1] // ret_heads
     ret_value = rv.shape[1] // ret_heads
@@ -746,9 +767,9 @@
             device_id_type=MESH,
         )
 
-    def add_own(out_ref, in_ref, half):
+    def add_own(out_ref, in_ref, half, res_ref):
         own = out_ref[pl.ds(pl.multiple_of(tp * half, half), half), :]
-        in_ref[...] = (own.astype(F32) + in_ref[...].astype(F32)).astype(BF)
+        res_ref[...] = (own.astype(F32) + in_ref[...].astype(F32)).astype(BF)
 
     token_swap = to_partner(gt, gt_in, half_tok, 0)
     token_swap.start()
@@ -775,30 +796,31 @@
             device_id_type=MESH,
         )
 
-    def column_reduce(c, i):
-        other = lax.rem(my_z + i, depth)
-        return pltpu.make_async_remote_copy(
-            src_ref=p1_sum.at[c, other],
-            dst_ref=p2_in.at[c, i - 1],
+    side = jnp.where(upper, 1, 0)
+
+    def column_reduce(c, which, slot, t):
+        return pltpu.make_async_remote_copy(
+            src_ref=p1_sum.at[c, which, t],
+            dst_ref=p2_in.at[c, t, slot],
             send_sem=p2_send.at[c],
-            recv_sem=p2_recv.at[c],
-            device_id={"st": other * PLANE + my_q},
-            device_id_type=MESH,
-        )
-
-    def column_gather(c, up, z):
-        at = kg.at[c, my_q * depth + z]
+            recv_sem=p2_recv.at[c, t],
+            device_id={"st": (1 + which) * PLANE + my_q},
+            device_id_type=MESH,
+        )
+
+    def column_gather(c, z, which, t):
+        at = kg.at[c, my_q * depth + 2 * which + t]
         return pltpu.make_async_remote_copy(
             src_ref=at,
             dst_ref=at,
-            send_sem=p3_send.at[up, c],
-            recv_sem=p3_recv.at[c, z],
-            device_id={"st": me + (2 * up - 1) * PLANE},
-            device_id_type=MESH,
-        )
-
-    def plane_gather(c, i, z):
-        at = kg.at[c, my_q * depth + z]
+            send_sem=p3_send.at[c],
+            recv_sem=p3_recv.at[c, 2 * which + t],
+            device_id={"st": z * PLANE + my_q},
+            device_id_type=MESH,
+        )
+
+    def plane_gather(c, i, which, t):
+        at = kg.at[c, my_q * depth + 2 * which + t]
         return pltpu.make_async_remote_copy(
             src_ref=at,
             dst_ref=at,
@@ -808,152 +830,178 @@
             device_id_type=MESH,
         )
 
+    def rows_of(p):
+        return pl.ds(pl.multiple_of(p * plen, plen), plen)
+
     def send_part(at, dst, sem, z):
         return pltpu.make_async_remote_copy(
-            src_ref=vp_out.at[at],
+            src_ref=at,
             dst_ref=dst,
             send_sem=vp_send.at[0],
-            recv_sem=vp_recv.at[sem],
+            recv_sem=sem,
             device_id={"st": z * PLANE + my_q},
             device_id_type=MESH,
         )
 
-    def merge(z, out_ref, *more):
-        def body(p, carry):
-            at = pl.ds(pl.multiple_of(p * plen, plen), plen)
-            acc = jnp.zeros((plen, HEAD), F32)
-            for r in range(PLANE):
-                row = req_in[my_z * PLANE + r, pl.ds(z, 1), :]
-                acc = acc + names(row, p, HEAD) * v_in[z, r].astype(F32)
-            for ref in more:
-                acc = acc + ref[at, :].astype(F32)
-            out_ref[at, :] = acc.astype(BF)
-            return carry
-
-        lax.fori_loop(0, pass_dev, body, 0)
+    def merge(z, p, *more):
+        acc = jnp.zeros((plen, HEAD), F32)
+        for r in range(PLANE):
+            row = req_in[my_z * PLANE + r, pl.ds(z, 1), :]
+            acc = acc + names(row, p, HEAD) * v_in[z, r].astype(F32)
+        for ref in more:
+            acc = acc + ref[rows_of(p), :].astype(F32)
+        return acc.astype(BF)
 
     def pass_near():
         z = jnp.where(is_end, near_mid, near_end)
-        merge(z, vp_out.at[2])
-        send_part(2, v_add.at[0], 2, z).start()
+
+        def body(p, carry):
+            vp_out[2, rows_of(p), :] = merge(z, p)
+            return carry
+
+        lax.fori_loop(0, pass_dev, body, 0)
+        send_part(vp_out.at[2], v_add.at[0], vp_recv.at[0], z).start()
 
     def pass_first(which):
         z = (far_mid, far_end)[which]
 
         @pl.when(is_end)
         def _():
-            merge(z, vp_out.at[which])
-            send_part(which, v_mid.at[which], which, near_mid).start()
+            def body(p, carry):
+                vp_out[which, rows_of(p), :] = merge(z, p)
+                send_part(
+                    vp_out.at[which, rows_of(p)],
+                    v_mid.at[which, rows_of(p)],
+                    vm_recv.at[which, p],
+                    near_mid,
+                ).start()
+                return carry
+
+            lax.fori_loop(0, pass_dev, body, 0)
 
     def pass_second(which):
         z = (far_mid, far_end)[which]
 
         @pl.when(jnp.logical_not(is_end))
         def _():
-            bulk(v_mid.at[which], vp_send.at[0], vp_recv.at[which]).wait_recv()
-            merge(z, vp_out.at[which], v_mid.at[which])
-            send_part(which, v_add.at[1], 3, z).start()
+            def body(p, carry):
+                at = v_mid.at[which, rows_of(p)]
+                bulk(at, vp_send.at[0], vm_recv.at[which, p]).wait_recv()
+                vp_out[which, rows_of(p), :] = merge(z, p, v_mid.at[which])
+                send_part(
+                    vp_out.at[which, rows_of(p)],
+                    v_add.at[1, rows_of(p)],
+                    vp_recv.at[1],
+                    z,
+                ).start()
+                return carry
+
+            lax.fori_loop(0, pass_dev, body, 0)
 
     rows_swapped.wait_recv()
     asked_far.wait_recv()
 
     own_cols = pl.ds(pl.multiple_of(my_q * quarter, quarter), quarter)
-    own_terms = []
-    for c in range(PARTS):
+    v_half = [bulk(gv_out.at[pl.ds(0, 2 * (PLANE - 1))], v_send.at[h], v_recv.at[h]) for h in range(2)]
+    def gather_keys(c):
         bulk_all(*gks[c]).wait_recv()
         if c == 0:
             start_some(1, n, *gks[1])
         gather_sum(gk_in.at[c], pk.at[c])
         for i in range(1, PLANE):
             share_key(c, i).start()
-        own_terms.append(tn(store[:, own_cols], pk[c]))
-        if c == 0:
-            for z in (near_mid, near_end):
-                for i in range(1, PLANE):
-                    hand_value(z, i, 1).start()
-    v_half = [bulk(gv_out.at[pl.ds(0, 2 * (PLANE - 1))], v_send.at[h], v_recv.at[h]) for h in range(2)]
-
-    token_swap.wait_recv()
-    add_own(gt, gt_in, half_tok)
-    token_out = pltpu.make_async_copy(gt_in, gt_hbm, out_sem.at[0])
-    token_out.start()
-
-    for c in range(PARTS):
+
+    def key_terms(c):
+        own = tn(store[:, own_cols], pk[c])
         bulk(pk_in.at[c], pk_send.at[c], pk_recv.at[c]).wait_recv()
         for part in range(2):
-            acc = own_terms[c][part * share : (part + 1) * share]
+            acc = own[part * share : (part + 1) * share]
             for i in range(1, PLANE):
                 acc = acc + tn(slices[part, i - 1], pk_in[c, i - 1])
-            acc = acc.reshape(depth // 2, -1, SPAN)
-            p1_sum[c, part * depth // 2 : (part + 1) * depth // 2] = acc.astype(BF)
-        for i in range(1, depth):
-            column_reduce(c, i).start()
-        if c == 0:
-            v_half[0].wait_recv()
-            pass_first(0)
-
-    def key_store_grad(i, carry):
-        rows = pl.ds(pl.multiple_of(i * TILE, TILE), TILE)
-        keys = jnp.concatenate([pk[c] for c in range(PARTS)], axis=1)
-        gs_key[:, rows] = nt(keys, wk[rows, :])
-        return carry
-
-    lax.fori_loop(0, width // TILE, key_store_grad, 0)
-
-    for c in range(PARTS):
-        bulk(p2_in.at[c], p2_send.at[c], p2_recv.at[c]).wait_recv()
-        acc = p1_sum[c, my_z].astype(F32)
-        for i in range(1, depth):
-            acc = acc + p2_in[c, i - 1].astype(F32)
-        kg[c, my_q * depth + my_z] = acc.astype(BF)
-
-        @pl.when(has_up)
+            p1_sum[c, part] = acc.astype(BF).reshape(p1_sum.shape[2:])
+
+        @pl.when(is_end)
         def _():
-            column_gather(c, 1, my_z).start()
-
-        @pl.when(has_down)
+            for t in range(2):
+                column_reduce(c, 1 - side, 2, t).start()
+                column_reduce(c, side, 0, t).start()
+
+        @pl.when(jnp.logical_not(is_end))
         def _():
-            column_gather(c, 0, my_z).start()
-
-        for i in range(1, PLANE):
-            plane_gather(c, i, my_z).start()
-        if c == 0:
-            pass_first(1)
-            pass_second(0)
-
+            for t in range(2):
+                column_reduce(c, 1 - side, 1, t).start()
+
+    def reduce_keys(c):
+        @pl.when(jnp.logical_not(is_end))
+        def _():
+            for t in range(2):
+                bulk(p2_in.at[c, t], p2_send.at[c], p2_recv.at[c, t]).wait_recv()
+                acc = p1_sum[c, side, t].astype(F32)
+                for i in range(depth - 1):
+                    acc = acc + p2_in[c, t, i].astype(F32)
+                kg[c, my_q * depth + 2 * side + t] = acc.astype(BF)
+                for z in (far_end, far_mid, near_end):
+                    column_gather(c, z, side, t).start()
+                for i in range(1, PLANE):
+                    plane_gather(c, i, side, t).start()
+
+    def hand_near():
+        for z in (near_mid, near_end):
+            for i in range(1, PLANE):
+                hand_value(z, i, 1).start()
+
+    def finish_tokens():
+        token_swap.wait_recv()
+        add_own(gt, gt_in, half_tok, gt_res)
+
+    gather_keys(0)
+    hand_near()
+    v_half[0].wait_recv()
+    pass_first(1)
+    finish_tokens()
+    key_terms(0)
+    gather_keys(1)
+    reduce_keys(0)
+    key_terms(1)
+    pass_first(0)
+    pass_second(1)
+    reduce_keys(1)
     v_half[1].wait_recv()
     pass_near()
-
-    def relay(step, carry):
-        k = 1 + lax.div(step, 2 * PARTS)
-        c = lax.rem(lax.div(step, 2), PARTS)
-        up = lax.rem(step, 2)
-        z = my_z + k * (1 - 2 * up)
-
-        @pl.when((z >= 0) & (z < depth))
-        def _():
-            column_gather(c, up, z).wait_recv()
-
-            @pl.when(jnp.where(up == 1, has_up, has_down))
-            def _():
-                column_gather(c, up, z).start()
-
-            for i in range(1, PLANE):
-                plane_gather(c, i, z).start()
-
-        return carry
-
-    lax.fori_loop(0, 2 * PARTS, relay, 0)
-    pass_second(1)
-    lax.fori_loop(2 * PARTS, 2 * PARTS * (depth - 1), relay, 0)
-
-    for sem in range(2):
-        bulk(v_add.at[sem], vp_send.at[0], vp_recv.at[2 + sem]).wait_recv()
-    merge(my_z, pv, v_add.at[0], v_add.at[1])
     wide = width // SWAPS
 
     def cut(i):
         return pl.ds(pl.multiple_of(i * wide, wide), wide)
+
+    def fan_out(c, at):
+        def body(s, carry):
+            keys = jnp.concatenate([pk[e] for e in range(PARTS)], axis=1)
+            gs_key[:, cut(at + s)] = nt(keys, wk[cut(at + s), :])
+            which = jnp.where(s == 0, side, 1 - side)
+
+            @pl.when(is_end | (s == 1))
+            def _():
+                for t in range(2):
+                    column_gather(c, my_z, which, t).wait_recv()
+                    for i in range(1, PLANE):
+                        plane_gather(c, i, which, t).start()
+
+            return carry
+
+        lax.fori_loop(0, 2, body, 0)
+
+    fan_out(0, 0)
+    pass_second(0)
+    fan_out(1, 2)
+
+    for sem in range(2):
+        bulk(v_add.at[sem], vp_send.at[0], vp_recv.at[sem]).wait_recv()
+
+    def merge_own(p, carry):
+        pv[rows_of(p), :] = merge(my_z, p, v_add.at[0], v_add.at[1])
+        return carry
+
+    lax.fori_loop(0, pass_dev, merge_own, 0)
 
     def half_of(which):
         return pl.ds(pl.multiple_of(which * half_store, half_store), half_store)
@@ -978,18 +1026,13 @@
     def store_sum(i, carry):
         store_swap(i).wait_recv()
         own = gs[half_of(tp), cut(i)]
-        gs_in[:, cut(i)] = (own.astype(F32) + gs_in[:, cut(i)].astype(F32)).astype(BF)
+        gs_res[:, cut(i)] = (own.astype(F32) + gs_in[:, cut(i)].astype(F32)).astype(BF)
         return carry
 
     lax.fori_loop(0, SWAPS, store_sum, 0)
-    store_out = pltpu.make_async_copy(gs_in, gs_hbm, out_sem.at[1])
-    store_out.start()
-
-    weight_out = []
     for c in range(PARTS):
         bulk(kg.at[c, pl.ds(0, n - depth)], p4_send.at[c], p4_recv.at[c]).wait_recv()
-        weight_out.append(pltpu.make_async_copy(kg.at[c], gkw_hbm.at[c], out_sem.at[2 + c]))
-        weight_out[c].start()
+        gkw_res[:, c * SPAN : (c + 1) * SPAN] = kg[c].reshape(width, SPAN).astype(F32)
 
     asked_near.wait_send()
     asked_far.wait_send()
@@ -1014,54 +1057,29 @@
         bulk_all(*gks[c]).wait_send()
         bulk(pk_in.at[c], pk_send.at[c], pk_recv.at[c]).wait_send()
         bulk(kg.at[c, pl.ds(0, n - depth)], p4_send.at[c], p4_recv.at[c]).wait_send()
-        bulk(p2_in.at[c], p2_send.at[c], p2_recv.at[c]).wait_send()
-    for z in range(depth):
-
-        @pl.when(my_z == z)
+    for c in range(PARTS):
+
+        @pl.when(is_end)
         def _():
-            for c in range(PARTS):
-                if z < depth - 1:
-                    at = kg.at[c, pl.ds(0, z + 1)]
-                    bulk(at, p3_send.at[1, c], p3_recv.at[c, 0]).wait_send()
-                if z > 0:
-                    at = kg.at[c, pl.ds(0, depth - z)]
-                    bulk(at, p3_send.at[0, c], p3_recv.at[c, 0]).wait_send()
+            bulk(kg.at[c, pl.ds(0, 4)], p2_send.at[c], p4_recv.at[c]).wait_send()
+
+        @pl.when(jnp.logical_not(is_end))
+        def _():
+            bulk(kg.at[c, pl.ds(0, 2)], p2_send.at[c], p4_recv.at[c]).wait_send()
+            bulk(kg.at[c, pl.ds(0, 6)], p3_send.at[c], p4_recv.at[c]).wait_send()
 
     rows_shared.wait_send()
     rows_swap.wait_send()
-    token_out.wait()
-    store_out.wait()
-    for out in weight_out:
-        out.wait()
-
-
-def finish_kernel(gt_hbm, gs_hbm, kg_hbm, ot_hbm, os_hbm, ok_hbm, gt, gs, kg, out, in_sem, out_sem):
-    pieces = in_sem.shape[0] - 2
-    span = out.shape[0] // pieces
-    cuts = [pl.ds(i * span, span) for i in range(pieces)]
-    loads = [
-        pltpu.make_async_copy(kg_hbm.at[:, at], kg.at[:, at], in_sem.at[i])
-        for i, at in enumerate(cuts)
+
+
+def finish_kernel(gt, gs, kg, ot, os, ok, sem):
+    copies = [
+        pltpu.make_async_copy(a, b, sem.at[i]) for i, (a, b) in enumerate(((kg, ok), (gt, ot), (gs, os)))
     ]
-    loads += [
-        pltpu.make_async_copy(gt_hbm, gt, in_sem.at[pieces]),
-        pltpu.make_async_copy(gs_hbm, gs, in_sem.at[pieces + 1]),
-    ]
-    for load in loads:
-        load.start()
-    stores = []
-    for i, at in enumerate(cuts):
-        loads[i].wait()
-        for c in range(PARTS):
-            out[at, c * SPAN : (c + 1) * SPAN] = kg[c, at, :].astype(F32)
-        stores.append(pltpu.make_async_copy(out.at[at], ok_hbm.at[at], out_sem.at[i]))
-        stores[-1].start()
-    for i, (a, b) in enumerate(((gt, ot_hbm), (gs, os_hbm))):
-        loads[pieces + i].wait()
-        stores.append(pltpu.make_async_copy(a, b, out_sem.at[pieces + i]))
-        stores[-1].start()
-    for store in stores:
-        store.wait()
+    for copy in copies:
+        copy.start()
+    for copy in copies:
+        copy.wait()
 
 
 def per_device(sizes, *args):
@@ -1093,14 +1111,19 @@
         return pltpu.VMEM(shape, dtype)
 
     any_spec = pl.BlockSpec(memory_space=pl.ANY)
-    smem = pl.BlockSpec(memory_space=pltpu.SMEM)
     vmem = pl.BlockSpec(memory_space=pltpu.VMEM)
     dma = pltpu.SemaphoreType.DMA
     like = [vm(*x.shape) for x in (tokens,)] + [vm(rows, width)]
     like += [vm(*x.shape) for x in (wq, wk, wv, wrq, wrk, wrv, og)]
     qs = [vm(length, w.shape[1]) for w in (wq, wrq, wrk, wrv)]
     scratch = (
-        like
+        [
+            pltpu.SMEM(ids.shape, jnp.int32),
+            pltpu.SMEM(rate.shape, F32),
+            vm(1, gain.shape[0], dtype=F32),
+            vm(1, gate.shape[0], dtype=F32),
+        ]
+        + like
         + qs
         + qs
         + [
@@ -1130,38 +1153,38 @@
             vm(rows, HEAD),
             vm(2, PLANE - 1, rows, width // (2 * PLANE)),
             vm(PARTS, PLANE - 1, rows, SPAN),
-            vm(PARTS, depth, piece, SPAN),
-            vm(PARTS, depth - 1, piece, SPAN),
+            vm(PARTS, 2, 2, piece, SPAN),
+            vm(PARTS, 2, depth - 1, piece, SPAN),
             vm(PARTS, n, piece, SPAN),
             pltpu.SMEM((n,), jnp.int32),
             pltpu.SMEM((n,), jnp.int32),
             pltpu.SMEM((n,), jnp.int32),
             dma((9,)),
-            dma((2 + PARTS,)),
+            dma((4,)),
         ]
         + [dma((1 + SWAPS,))] * 2
         + [dma((2,))] * 2
         + [dma((2,))] * 2
-        + [dma((1,)), dma((4,))]
+        + [dma((1,)), dma((2,)), dma((2, pass_dev))]
         + [dma((PARTS,))] * 2
         + [dma((2, depth)), dma((depth, CHUNKS))]
         + [dma((1,))] * 6
-        + [dma((PARTS,))] * 4
-        + [dma((2, PARTS)), dma((PARTS, depth))]
+        + [dma((PARTS,))] * 3
+        + [dma((PARTS, 2)), dma((PARTS,)), dma((PARTS, 4))]
         + [dma((PARTS,))] * 2
     )
     grad_tokens, grad_store, grad_key = pl.pallas_call(
         functools.partial(fused_kernel, n),
         out_shape=(
-            jax.ShapeDtypeStruct((length // 2, width), BF),
-            jax.ShapeDtypeStruct((rows // 2, width), BF),
-            jax.ShapeDtypeStruct((PARTS, n, piece, SPAN), BF),
+            pltpu.VMEM((length // 2, width), BF),
+            pltpu.VMEM((rows // 2, width), BF),
+            pltpu.VMEM((width, HEAD), F32),
         ),
-        in_specs=[smem, smem, vmem, vmem] + [any_spec] * 9,
-        out_specs=(any_spec, any_spec, any_spec),
+        in_specs=[any_spec] * 13,
+        out_specs=(vmem, vmem, vmem),
         scratch_shapes=scratch,
         compiler_params=pltpu.CompilerParams(
-            collective_id=0, has_side_effects=True, vmem_limit_bytes=60 * 2**20
+            collective_id=0, has_side_effects=True, vmem_limit_bytes=VMEM_BYTES - (length + rows + 4 * HEAD) * width - 2**16
         ),
     )(
         ids,
@@ -1185,17 +1208,11 @@
             jax.ShapeDtypeStruct((rows // 2, width), BF),
             jax.ShapeDtypeStruct((width, HEAD), F32),
         ),
-        in_specs=[any_spec] * 3,
+        in_specs=[vmem] * 3,
         out_specs=(any_spec, any_spec, any_spec),
-        scratch_shapes=[
-            vm(length // 2, width),
-            vm(rows // 2, width),
-            vm(PARTS, width, SPAN),
-            vm(width, HEAD, dtype=F32),
-            dma((6,)),
-            dma((6,)),
-        ],
-    )(grad_tokens, grad_store, grad_key.reshape(PARTS, width, SPAN))
+        scratch_shapes=[dma((3,))],
+        compiler_params=pltpu.CompilerParams(vmem_limit_bytes=8 * 2**20),
+    )(grad_tokens, grad_store, grad_key)
     return (grad_tokens, grad_store.reshape(pass_dev // 2, plen, width), grad_key)
 
 

time: 73.9 us -> 68.6 us (0.928)
  Pallas kernels: 73 us -> 67.8 us
    pallas_call x1, Pallas kernels: 70.3 us -> 66.1 us  [per_device(): pl.pallas_call(functools.partial(fused_kernel, n), out_shape=(pltpu.VMEM(...]
    pallas_call x1, Pallas kernels: 2.75 us -> 1.68 us  [per_device(): pl.pallas_call(finish_kernel, out_shape=(jax.ShapeDtypeStruct((length //...]
where the time goes in v3:
time: 68.6 us; the launch traced here: 68.4 us
  Pallas kernels  67.8 us (99%)
    pallas_call x1, Pallas kernels, per_device(): pl.pallas_call(functools.partial(fused_kernel, n), out_shape=(pltpu.VMEM(...  66.1 us
    pallas_call x1, Pallas kernels, per_device(): pl.pallas_call(finish_kernel, out_shape=(jax.ShapeDtypeStruct((length //...  1.68 us

profile of v3, /device:TPU:0, one launch (start us, length us, event | category | flops | bytes accessed | tf_op | source)
XLA Modules:
  0.0 68.4 jit_solution(2052131333903049316)
XLA Ops:
  0.6 66.1 %shard_map.148 = (bf16[128,2048]{1,0:T(8,128)(2,1)S(1)}, bf16[128,2048]{1,0:T(8,128)(2,1)S(1)}, f32[2048,256]{1,0:T(8,128)S(1)}) custom-call(s32[4,4]{1,0:T(4,128)} %ids_hbm.1, f32[4]{0:T(128)} %rate_hbm.1, f32[1,1024]{1,0:T(1,128)} %bitcast.5, f32[1,1024]{1,0:T(1,128)} %bitcast.6, bf16[256,2048]{1,0:T(8,128)(2,1)} %tokens_hbm.1, bf16[256,2048]{1,0:T(8,128)(2,1)} %bitcast.4, ...), custom_call_target="tpu_custom_call" | custom-call | tf_op jit(solution)/shard_map/pallas_call | solution.py:1176
  66.7 1.7 %shard_map.149 = (bf16[128,2048]{1,0:T(8,128)(2,1)}, bf16[128,2048]{1,0:T(8,128)(2,1)}, f32[2048,256]{1,0:T(8,128)}) custom-call(bf16[128,2048]{1,0:T(8,128)(2,1)S(1)} %get-tuple-element.9.gt, bf16[128,2048]{1,0:T(8,128)(2,1)S(1)} %get-tuple-element.10.gs, f32[2048,256]{1,0:T(8,128)S(1)} %get-tuple-element.11.kg), custom_call_target="tpu_custom_call" | custom-call | tf_op jit(solution)/shard_map/pallas_call | solution.py:1204

commit v4 on v3

--- a/solution.py
+++ b/solution.py
@@ -219,7 +219,7 @@
 PARTS = 2
 SPAN = 128
 CHUNKS = 4
-SWAPS = 4
+SWAPS = 2
 TOGETHER = 4
 VMEM_BYTES = 67043328
 TILE = 256
@@ -747,15 +747,16 @@
     for z in range(depth):
         v_in[z, my_q] = gv_out[z * PLANE + my_q]
 
+    for z in (far_end, far_mid):
+        for i in range(1, PLANE):
+            hand_value(z, i, 0).start()
+
     def finish_total(i, carry):
         rows = pl.ds(pl.multiple_of(i * TILE, TILE), TILE)
         gt[:, rows] = (total[:, rows] + nt(gq[...], wq[rows, :])).astype(BF)
         return carry
 
     lax.fori_loop(0, width // TILE, finish_total, 0)
-    for z in (far_end, far_mid):
-        for i in range(1, PLANE):
-            hand_value(z, i, 0).start()
 
     def to_partner(out_ref, in_ref, half, at):
         return pltpu.make_async_remote_copy(
@@ -965,18 +966,22 @@
     key_terms(1)
     pass_first(0)
     pass_second(1)
+    wide = width // SWAPS
+
+    def cut(i):
+        return pl.ds(pl.multiple_of(i * wide, wide), wide)
+
+    def key_store_grad(i, carry):
+        keys = jnp.concatenate([pk[e] for e in range(PARTS)], axis=1)
+        gs_key[:, cut(i)] = nt(keys, wk[cut(i), :])
+        return carry
+
+    lax.fori_loop(0, SWAPS, key_store_grad, 0)
     reduce_keys(1)
     v_half[1].wait_recv()
     pass_near()
-    wide = width // SWAPS
-
-    def cut(i):
-        return pl.ds(pl.multiple_of(i * wide, wide), wide)
-
-    def fan_out(c, at):
+    def fan_out(c):
         def body(s, carry):
-            keys = jnp.concatenate([pk[e] for e in range(PARTS)], axis=1)
-            gs_key[:, cut(at + s)] = nt(keys, wk[cut(at + s), :])
             which = jnp.where(s == 0, side, 1 - side)
 
             @pl.when(is_end | (s == 1))
@@ -990,9 +995,9 @@
 
         lax.fori_loop(0, 2, body, 0)
 
-    fan_out(0, 0)
+    fan_out(0)
     pass_second(0)
-    fan_out(1, 2)
+    fan_out(1)
 
     for sem in range(2):
         bulk(v_add.at[sem], vp_send.at[0], vp_recv.at[sem]).wait_recv()
@@ -1073,9 +1078,10 @@
 
 
 def finish_kernel(gt, gs, kg, ot, os, ok, sem):
-    copies = [
-        pltpu.make_async_copy(a, b, sem.at[i]) for i, (a, b) in enumerate(((kg, ok), (gt, ot), (gs, os)))
-    ]
+    span = kg.shape[0] // 4
+    pairs = [(kg.at[pl.ds(i * span, span)], ok.at[pl.ds(i * span, span)]) for i in range(4)]
+    pairs += [(gt, ot), (gs, os)]
+    copies = [pltpu.make_async_copy(a, b, sem.at[i]) for i, (a, b) in enumerate(pairs)]
     for copy in copies:
         copy.start()
     for copy in copies:
@@ -1210,7 +1216,7 @@
         ),
         in_specs=[vmem] * 3,
         out_specs=(any_spec, any_spec, any_spec),
-        scratch_shapes=[dma((3,))],
+        scratch_shapes=[dma((6,))],
         compiler_params=pltpu.CompilerParams(vmem_limit_bytes=8 * 2**20),
     )(grad_tokens, grad_store, grad_key)
     return (grad_tokens, grad_store.reshape(pass_dev // 2, plen, width), grad_key)

time: 68.6 us -> 68.5 us (level)
  no operation moved by 1% of the time
where the time goes in v4:
time: 68.5 us; the launch traced here: 68.3 us
  Pallas kernels  67.7 us (99%)
    pallas_call x1, Pallas kernels, per_device(): pl.pallas_call(functools.partial(fused_kernel, n), out_shape=(pltpu.VMEM(...  66 us
    pallas_call x1, Pallas kernels, per_device(): pl.pallas_call(finish_kernel, out_shape=(jax.ShapeDtypeStruct((length //...  1.71 us

profile of v4, /device:TPU:0, one launch (start us, length us, event | category | flops | bytes accessed | tf_op | source)
XLA Modules:
  0.0 68.3 jit_solution(1989247985135570235)
XLA Ops:
  0.6 66.0 %shard_map.148 = (bf16[128,2048]{1,0:T(8,128)(2,1)S(1)}, bf16[128,2048]{1,0:T(8,128)(2,1)S(1)}, f32[2048,256]{1,0:T(8,128)S(1)}) custom-call(s32[4,4]{1,0:T(4,128)} %ids_hbm.1, f32[4]{0:T(128)} %rate_hbm.1, f32[1,1024]{1,0:T(1,128)} %bitcast.5, f32[1,1024]{1,0:T(1,128)} %bitcast.6, bf16[256,2048]{1,0:T(8,128)(2,1)} %tokens_hbm.1, bf16[256,2048]{1,0:T(8,128)(2,1)} %bitcast.4, ...), custom_call_target="tpu_custom_call" | custom-call | tf_op jit(solution)/shard_map/pallas_call | solution.py:1182
  66.6 1.7 %shard_map.149 = (bf16[128,2048]{1,0:T(8,128)(2,1)}, bf16[128,2048]{1,0:T(8,128)(2,1)}, f32[2048,256]{1,0:T(8,128)}) custom-call(bf16[128,2048]{1,0:T(8,128)(2,1)S(1)} %get-tuple-element.9.gt, bf16[128,2048]{1,0:T(8,128)(2,1)S(1)} %get-tuple-element.10.gs, f32[2048,256]{1,0:T(8,128)S(1)} %get-tuple-element.11.kg), custom_call_target="tpu_custom_call" | custom-call | tf_op jit(solution)/shard_map/pallas_call | solution.py:1210
